TPU v7x, 512 devices: a 4x2x32 block of a 4x8x32 slice. The times are simulated.
512 devices in a mesh: grp: 2 (over y), kv: 32 (over z), tp: 8 (over x, core).
Axes of the slice: x: 4, y: 2, z: 32, core: 2. Of those that a mesh axis runs over, the one named last changes fastest.
The devices are a block of a 4x8x32 slice.
Arguments:
- tokens: bfloat16 [256, 2048], P('grp', ('kv', 'tp')), parts along dimension 0, may hold values from -13 to 13, as said below
- state: float32 [256, 16, 128, 128], P(('grp', 'kv'), 'tp'), parts along dimension 0, may hold values from -0.6 to 0.6
- norm_gain: bfloat16 [2048], P('kv'), may hold values from 0.099609375 to 1.8984375
- w_query: bfloat16 [2048, 2048], P('kv', 'tp'), may hold values from -0.125 to 0.125
- w_key: bfloat16 [2048, 2048], P('kv', 'tp'), may hold values from -0.125 to 0.125
- w_value: bfloat16 [2048, 2048], P('kv', 'tp'), may hold values from -0.125 to 0.125
- w_beta: bfloat16 [2048, 16], replicated, may hold values from -0.125 to 0.125
- w_decay: bfloat16 [2048, 16], replicated, may hold values from -0.125 to 0.125
- a_log: float32 [16], P('tp'), may hold values from -3 to 1
- dt_bias: float32 [16], P('tp'), may hold values from -2 to 1
- head_gain: float32 [128], replicated, may hold values from 0.1 to 1.9
- w_out: bfloat16 [2048, 2048], P('tp', 'kv'), may hold values from -0.125 to 0.125
- mixer_gain: bfloat16 [2048], P('kv'), may hold values from 0.099609375 to 1.8984375
- w_up: bfloat16 [2048, 8192], P('kv', 'tp'), may hold values from -0.125 to 0.125
- w_down: bfloat16 [8192, 2048], P('tp', 'kv'), may hold values from -0.0625 to 0.0625
Outputs:
- mixed: bfloat16 [256, 2048], P('grp', ('kv', 'tp')), parts along dimension 0
- new_state: float32 [256, 16, 128, 128], P(('grp', 'kv'), 'tp'), parts along dimension 0
There are 2 independent parts, one for each index of `grp`. A program takes and returns all parts, laid end to end along the dimension named above; an argument that names none is the same for every part. Nothing has to cross between parts.
Inputs may be any that keep to these rules, and one draw needn't show every extreme that they name: `tokens`: activations of order one.
All inputs are finite; a program needn't handle non-finite values.
Results may differ from a plain program's by a relative error of at most 0.019.
Values may be sent and summed in bfloat16 or wider, within the bound.
A program may use at most 64 MiB of HBM per device.

v0:
```python
import jax
import jax.numpy as jnp
from jax import lax
from jax.sharding import PartitionSpec as P

D = 2048


epsilon = 1e-06


def joined_along(parts, dim):
    shape = list(parts.shape[1:])
    shape[dim] *= parts.shape[0]
    return jnp.moveaxis(parts, 0, dim).reshape(shape)


def from_everyone(x, axis):
    copies = jnp.broadcast_to(x, (lax.axis_size(axis), *x.shape))
    return lax.all_to_all(copies, axis, split_axis=0, concat_axis=0, tiled=True)


def gather_directly(x, axis, dim):
    return joined_along(from_everyone(x, axis), dim)


def split_up(x, dim, devices):
    before, after = (x.shape[:dim], x.shape[dim + 1 :])
    return jnp.moveaxis(x.reshape(*before, devices, -1, *after), dim, 0)


def sent_and_summed(x, axis, dim):
    parts = split_up(x, dim, lax.axis_size(axis))
    arrived = lax.all_to_all(parts, axis, split_axis=0, concat_axis=0, tiled=True)
    return arrived.sum(axis=0)


def in_one_piece(arrays, axis, dim, along):
    columns = [a.reshape(*a.shape[:along], -1) for a in arrays]
    both = jnp.concatenate(columns, axis=along)
    whole, at, done = (sent_and_summed(both, axis, dim), 0, [])
    for a, column in zip(arrays, columns):
        section = whole[..., at : at + column.shape[along]]
        done.append(section.reshape(*section.shape[:along], *a.shape[along:]))
        at += column.shape[along]
    return tuple(done)


def summed_on_arrival(x, axis, dim):
    parts = split_up(x, dim, lax.axis_size(axis))
    arrived = lax.all_to_all(parts, axis, split_axis=0, concat_axis=0, tiled=True)
    return arrived.astype(jnp.float32).sum(axis=0)


def taken_together(x, axis):
    everything = from_everyone(x, axis)
    return jnp.sum(everything, axis=0)


def dotted(left, right):
    return jnp.dot(left, right, preferred_element_type=jnp.float32)


def delta_update(
    query_pre, key_pre, value_pre, beta_pre, decay_pre, state, a_log, dt_bias, head_gain
):
    query = query_pre * lax.rsqrt(jnp.sum(query_pre * query_pre, axis=-1, keepdims=True) + epsilon)
    keyed = key_pre * lax.rsqrt(jnp.sum(key_pre * key_pre, axis=-1, keepdims=True) + epsilon)
    beta = jax.nn.sigmoid(beta_pre)
    decay = jnp.exp(-jnp.exp(a_log) * jax.nn.softplus(decay_pre + dt_bias))
    key_read = jnp.einsum("bhk,bhkv->bhv", keyed, state)
    query_read = jnp.einsum("bhk,bhkv->bhv", query, state)
    fresh = beta[..., None] * (value_pre - decay[..., None] * key_read)
    new_state = decay[..., None, None] * state + keyed[..., :, None] * fresh[..., None, :]
    intersection = jnp.sum(query * keyed, axis=-1)
    reading = decay[..., None] * query_read + intersection[..., None] * fresh
    normed = (
        reading
        * lax.rsqrt(jnp.mean(reading * reading, axis=-1, keepdims=True) + epsilon)
        * head_gain
    )
    return (normed.astype(jnp.bfloat16), new_state)


def local(
    tokens,
    state,
    norm_gain,
    w_query,
    w_key,
    w_value,
    w_beta,
    w_decay,
    a_log,
    dt_bias,
    head_gain,
    w_out,
    mixer_gain,
    w_up,
    w_down,
):
    seq_here = state.shape[0]
    heads_here = state.shape[1]
    head_size = state.shape[2]
    kv_index = lax.axis_index("kv")
    tp_index = lax.axis_index("tp")
    gathered = gather_directly(tokens, "tp", 1)
    block = gathered.shape[1]
    inputs = gathered.astype(jnp.float32)
    scaled = (inputs * norm_gain.astype(jnp.float32)).astype(jnp.bfloat16)
    partial_sq = jnp.sum(inputs * inputs, axis=1)
    beta_rows = lax.dynamic_slice(
        w_beta, (kv_index * block, tp_index * heads_here), (block, heads_here)
    )
    decay_rows = lax.dynamic_slice(
        w_decay, (kv_index * block, tp_index * heads_here), (block, heads_here)
    )
    query_part = dotted(scaled, w_query)
    key_part = dotted(scaled, w_key)
    value_part = dotted(scaled, w_value)
    beta_part = dotted(scaled, beta_rows)
    decay_part = dotted(scaled, decay_rows)
    query_sum, key_sum, value_sum, beta_sum, decay_sum, square_sum = in_one_piece(
        (query_part, key_part, value_part, beta_part, decay_part, partial_sq), "kv", 0, 1
    )
    first = lax.rsqrt(square_sum / D + epsilon)[:, None]
    query_pre = (first * query_sum).reshape(seq_here, heads_here, head_size)
    key_pre = (first * key_sum).reshape(seq_here, heads_here, head_size)
    value_pre = (first * value_sum).reshape(seq_here, heads_here, head_size)
    normed, new_state = delta_update(
        query_pre,
        key_pre,
        value_pre,
        first * beta_sum,
        first * decay_sum,
        state,
        a_log,
        dt_bias,
        head_gain,
    )
    normed = normed.reshape(seq_here, heads_here * head_size)
    head_part = dotted(gather_directly(normed, "kv", 0), w_out)
    attended = summed_on_arrival(head_part.astype(jnp.bfloat16), "tp", 1)
    middle = (tokens.astype(jnp.float32) + attended).astype(jnp.bfloat16)
    middle_rows = gather_directly(middle, "tp", 1).astype(jnp.float32)
    square_two = taken_together(jnp.sum(middle_rows * middle_rows, axis=1), "kv")
    second = lax.rsqrt(square_two / D + epsilon)[:, None]
    scaled_two = (middle_rows * mixer_gain.astype(jnp.float32)).astype(jnp.bfloat16)
    up_part = dotted(scaled_two, w_up)
    up_share = sent_and_summed(up_part, "kv", 1)
    hidden_share = jnp.square(jax.nn.relu(second * up_share)).astype(jnp.bfloat16)
    down_part = dotted(gather_directly(hidden_share, "kv", 1), w_down)
    lowered = summed_on_arrival(down_part.astype(jnp.bfloat16), "tp", 1)
    mixed = (middle.astype(jnp.float32) + lowered).astype(jnp.bfloat16)
    return (mixed, new_state)


def solution(mesh):
    return jax.shard_map(
        local,
        mesh=mesh,
        in_specs=(
            P("grp", ("kv", "tp")),
            P(("grp", "kv"), "tp", None, None),
            P("kv"),
            P("kv", "tp"),
            P("kv", "tp"),
            P("kv", "tp"),
            P(),
            P(),
            P("tp"),
            P("tp"),
            P(),
            P("tp", "kv"),
            P("kv"),
            P("kv", "tp"),
            P("tp", "kv"),
        ),
        out_specs=(P("grp", ("kv", "tp")), P(("grp", "kv"), "tp", None, None)),
        check_vma=False,
    )
```

profile of v0, /device:TPU:33, one launch (start us, length us, event | category | flops | bytes accessed | tf_op | source)
XLA Modules:
  0.0 324.2 jit_solution(18350188781352569365)
XLA Ops:
  0.6 0.0 copy-start
  0.6 1.3 broadcast_in_dim.10
  2.0 44.7 %all-to-all-start = ((bf16[8,128,8]{1,2,0:T(8,128)(2,1)}), bf16[8,128,8]{1,2,0:T(8,128)(2,1)S(1)}, u32[]{:S(2)}, u32[]{:S(2)}) async-start(bf16[8,128,8]{1,2,0:T(8,128)(2,1)} %broadcast_in_dim.10), calls=%async_computation | async-start | bytes 32768 | tf_op jit(solution)/shard_map/all_to_all | solution.py:20
  46.7 0.7 copy-done.11
  47.3 4.1 %all-to-all-done = bf16[8,128,8]{1,2,0:T(8,128)(2,1)S(1)} async-done(((bf16[8,128,8]{1,2,0:T(8,128)(2,1)}), bf16[8,128,8]{1,2,0:T(8,128)(2,1)S(1)}, u32[]{:S(2)}, u32[]{:S(2)}) %all-to-all-start) | async-done | bytes 16416 | tf_op jit(solution)/shard_map/all_to_all | solution.py:20
  51.4 0.2 copy.142
  51.6 0.2 reshape.133
  51.8 0.7 copy-done.4
  52.6 0.1 fusion.10
  52.7 0.6 copy-done.5
  53.3 0.1 fusion.8
  53.5 0.6 copy-done.6
  54.1 0.1 fusion.6
  54.2 0.9 fusion.32
  55.1 0.9 fusion.30
  56.0 0.1 concatenate.6
  56.1 0.3 copy.146
  56.5 0.1 concatenate.7
  56.6 1.1 copy.147
  57.7 6.9 %all-to-all-start.1 = ((f32[32,4,773]{2,1,0:T(4,128)}), f32[32,4,773]{2,1,0:T(4,128)S(1)}, u32[]{:S(2)}, u32[]{:S(2)}) async-start(f32[32,4,773]{2,1,0:T(4,128)} %copy.147), calls=%async_computation.1 | async-start | bytes 917504 | tf_op jit(solution)/shard_map/all_to_all | solution.py:34
  64.6 57.9 %all-to-all-done.1 = f32[32,4,773]{2,1,0:T(4,128)S(1)} async-done(((f32[32,4,773]{2,1,0:T(4,128)}), f32[32,4,773]{2,1,0:T(4,128)S(1)}, u32[]{:S(2)}, u32[]{:S(2)}) %all-to-all-start.1) | async-done | bytes 395808 | tf_op jit(solution)/shard_map/all_to_all | solution.py:34
  122.5 0.1 reduce_sum.100
  122.5 0.2 fusion.29
  122.7 0.1 slice_multiply_fusion.1
  122.8 0.1 multiply_reduce_fusion.2
  122.9 0.1 multiply_reduce_fusion.3
  123.0 0.2 multiply_reduce_fusion.1
  123.2 0.1 copy.149
  123.3 0.6 copy-done.9
  123.9 0.1 fusion.25
  124.0 0.1 copy.148
  124.1 0.2 fusion.37
  124.2 0.2 fusion.38
  124.4 0.1 copy.150
  124.5 0.2 multiply_reduce_fusion
  124.7 0.1 copy.151
  124.8 0.1 copy.152
  124.9 0.7 copy-done.8
  125.5 0.1 fusion.19
  125.7 26.7 %all_to_all.46 = bf16[32,4,256]{2,1,0:T(4,128)(2,1)S(1)} all-to-all(bf16[32,4,256]{2,1,0:T(4,128)(2,1)S(1)} %broadcast_in_dim.11), channel_id=1, replica_groups=mesh['grp'=2,'kv'=32,'tp'=8] {'kv'}, dimensions={0} | all-to-all | bytes 131072 | tf_op jit(solution)/shard_map/all_to_all | solution.py:20
  152.4 0.7 copy-done.3
  153.1 0.1 fusion
  153.2 10.6 %all_to_all.47 = bf16[8,128,8]{1,2,0:T(8,128)(2,1)S(1)} all-to-all(bf16[8,128,8]{1,2,0:T(8,128)(2,1)S(1)} %fusion), channel_id=1, replica_groups=mesh['grp'=2,'kv'=32,'tp'=8] {'tp'}, dimensions={0} | all-to-all | bytes 32768 | tf_op jit(solution)/shard_map/all_to_all | solution.py:51
  163.8 0.7 copy-done.7
  164.5 0.6 broadcast_in_dim.12
  165.1 4.0 %all-to-all-start.4 = ((bf16[8,128,8]{1,2,0:T(8,128)(2,1)}), bf16[8,128,8]{1,2,0:T(8,128)(2,1)S(1)}, u32[]{:S(2)}, u32[]{:S(2)}) async-start(bf16[8,128,8]{1,2,0:T(8,128)(2,1)} %broadcast_in_dim.12), calls=%async_computation.4 | async-start | bytes 32768 | tf_op jit(solution)/shard_map/all_to_all | solution.py:20
  169.1 0.2 copy.154
  169.2 0.5 copy-done.10
  169.7 0.1 reshape.134
  169.8 4.0 %all-to-all-done.4 = bf16[8,128,8]{1,2,0:T(8,128)(2,1)S(1)} async-done(((bf16[8,128,8]{1,2,0:T(8,128)(2,1)}), bf16[8,128,8]{1,2,0:T(8,128)(2,1)S(1)}, u32[]{:S(2)}, u32[]{:S(2)}) %all-to-all-start.4) | async-done | bytes 16416 | tf_op jit(solution)/shard_map/all_to_all | solution.py:20
  173.8 0.6 broadcast_in_dim.13
  174.4 4.8 %all-to-all-start.5 = ((f32[32,1,128]{2,1,0:T(1,128)}), f32[32,1,128]{2,1,0:T(1,128)S(1)}, u32[]{:S(2)}, u32[]{:S(2)}) async-start(f32[32,1,128]{2,1,0:T(1,128)} %broadcast_in_dim.13), calls=%async_computation.5 | async-start | bytes 32768 | tf_op jit(solution)/shard_map/all_to_all | solution.py:20
  179.2 1.1 convolution_bitcast_fusion
  180.3 19.3 %all-to-all-done.5 = f32[32,1,128]{2,1,0:T(1,128)S(1)} async-done(((f32[32,1,128]{2,1,0:T(1,128)}), f32[32,1,128]{2,1,0:T(1,128)S(1)}, u32[]{:S(2)}, u32[]{:S(2)}) %all-to-all-start.5) | async-done | bytes 16416 | tf_op jit(solution)/shard_map/all_to_all | solution.py:20
  199.6 4.8 %all-to-all-start.6 = ((f32[32,128,32]{1,2,0:T(8,128)}), f32[32,128,32]{1,2,0:T(8,128)S(1)}, u32[]{:S(2)}, u32[]{:S(2)}) async-start(f32[32,128,32]{1,2,0:T(8,128)} %convolution_bitcast_fusion), calls=%async_computation.6 | async-start | bytes 1048576 | tf_op jit(solution)/shard_map/all_to_all | solution.py:34
  204.4 60.8 %all-to-all-done.6 = f32[32,128,32]{1,2,0:T(8,128)S(1)} async-done(((f32[32,128,32]{1,2,0:T(8,128)}), f32[32,128,32]{1,2,0:T(8,128)S(1)}, u32[]{:S(2)}, u32[]{:S(2)}) %all-to-all-start.6) | async-done | bytes 524320 | tf_op jit(solution)/shard_map/all_to_all | solution.py:34
  265.3 0.7 broadcast_in_dim.14
  266.0 6.1 %all-to-all-start.7 = ((bf16[32,128,32]{1,2,0:T(8,128)(2,1)}), bf16[32,128,32]{1,2,0:T(8,128)(2,1)S(1)}, u32[]{:S(2)}, u32[]{:S(2)}) async-start(bf16[32,128,32]{1,2,0:T(8,128)(2,1)} %broadcast_in_dim.14), calls=%async_computation.7 | async-start | bytes 524288 | tf_op jit(solution)/shard_map/all_to_all | solution.py:20
  272.1 37.3 %all-to-all-done.7 = bf16[32,128,32]{1,2,0:T(8,128)(2,1)S(1)} async-done(((bf16[32,128,32]{1,2,0:T(8,128)(2,1)}), bf16[32,128,32]{1,2,0:T(8,128)(2,1)S(1)}, u32[]{:S(2)}, u32[]{:S(2)}) %all-to-all-start.7) | async-done | bytes 262176 | tf_op jit(solution)/shard_map/all_to_all | solution.py:20
  309.5 0.8 fusion.1
  310.2 8.7 %all-to-all-start.8 = ((bf16[8,128,8]{1,2,0:T(8,128)(2,1)}), bf16[8,128,8]{1,2,0:T(8,128)(2,1)S(1)}, u32[]{:S(2)}, u32[]{:S(2)}) async-start(bf16[8,128,8]{1,2,0:T(8,128)(2,1)} %fusion.1), calls=%async_computation.8 | async-start | bytes 32768 | tf_op jit(solution)/shard_map/all_to_all | solution.py:51
  318.9 1.0 multiply_add_fusion
  319.9 3.7 %all-to-all-done.8 = bf16[8,128,8]{1,2,0:T(8,128)(2,1)S(1)} async-done(((bf16[8,128,8]{1,2,0:T(8,128)(2,1)}), bf16[8,128,8]{1,2,0:T(8,128)(2,1)S(1)}, u32[]{:S(2)}, u32[]{:S(2)}) %all-to-all-start.8) | async-done | bytes 16416 | tf_op jit(solution)/shard_map/all_to_all | solution.py:51
  323.6 0.6 add_convert_fusion
  (36 shorter events, 0.3 us)
Async XLA Ops:
  0.6 308.8 %copy-start = (bf16[1024,64]{0,1:T(8,128)(2,1)S(1)}, bf16[1024,64]{0,1:T(8,128)(2,1)}, u32[]{:S(2)}) copy-start(bf16[1024,64]{0,1:T(8,128)(2,1)} %param.29) | copy-start | bytes 393220
  2.0 49.4 %all-to-all-start = ((bf16[8,128,8]{1,2,0:T(8,128)(2,1)}), bf16[8,128,8]{1,2,0:T(8,128)(2,1)S(1)}, u32[]{:S(2)}, u32[]{:S(2)}) async-start(bf16[8,128,8]{1,2,0:T(8,128)(2,1)} %broadcast_in_dim.10), calls=%async_computation | async-start | bytes 32768 | tf_op jit(solution)/shard_map/all_to_all | solution.py:20
  46.7 0.7 copy-start.11
  51.8 0.8 copy-start.4
  52.6 0.8 copy-start.5
  53.3 0.8 copy-start.6
  57.6 6.9 %copy-start.12 = (f32[2]{0:T(128)S(1)}, f32[2]{0:T(128)}, u32[]{:S(2)}) copy-start(f32[2]{0:T(128)} %param.23) | copy-start | bytes 28
  57.7 66.4 %copy-start.1 = (f32[4,2,128,128]{3,2,1,0:T(8,128)S(1)}, f32[4,2,128,128]{3,2,1,0:T(8,128)}, u32[]{:S(2)}) copy-start(f32[4,2,128,128]{3,2,1,0:T(8,128)} %param.16) | copy-start | bytes 1572868
  57.7 64.8 %all-to-all-start.1 = ((f32[32,4,773]{2,1,0:T(4,128)}), f32[32,4,773]{2,1,0:T(4,128)S(1)}, u32[]{:S(2)}, u32[]{:S(2)}) async-start(f32[32,4,773]{2,1,0:T(4,128)} %copy.147), calls=%async_computation.1 | async-start | bytes 917504 | tf_op jit(solution)/shard_map/all_to_all | solution.py:34
  123.2 0.7 copy-start.9
  124.9 0.7 copy-start.8
  152.4 0.8 copy-start.3
  153.1 15.9 %copy-start.2 = (bf16[64,1024]{1,0:T(8,128)(2,1)S(1)}, bf16[64,1024]{1,0:T(8,128)(2,1)}, u32[]{:S(2)}) copy-start(bf16[64,1024]{1,0:T(8,128)(2,1)} %param.28) | copy-start | bytes 393220
  163.8 0.7 copy-start.7
  165.1 8.7 %all-to-all-start.4 = ((bf16[8,128,8]{1,2,0:T(8,128)(2,1)}), bf16[8,128,8]{1,2,0:T(8,128)(2,1)S(1)}, u32[]{:S(2)}, u32[]{:S(2)}) async-start(bf16[8,128,8]{1,2,0:T(8,128)(2,1)} %broadcast_in_dim.12), calls=%async_computation.4 | async-start | bytes 32768 | tf_op jit(solution)/shard_map/all_to_all | solution.py:20
  169.1 0.7 copy-start.10
  174.4 25.2 %all-to-all-start.5 = ((f32[32,1,128]{2,1,0:T(1,128)}), f32[32,1,128]{2,1,0:T(1,128)S(1)}, u32[]{:S(2)}, u32[]{:S(2)}) async-start(f32[32,1,128]{2,1,0:T(1,128)} %broadcast_in_dim.13), calls=%async_computation.5 | async-start | bytes 32768 | tf_op jit(solution)/shard_map/all_to_all | solution.py:20
  199.6 65.6 %all-to-all-start.6 = ((f32[32,128,32]{1,2,0:T(8,128)}), f32[32,128,32]{1,2,0:T(8,128)S(1)}, u32[]{:S(2)}, u32[]{:S(2)}) async-start(f32[32,128,32]{1,2,0:T(8,128)} %convolution_bitcast_fusion), calls=%async_computation.6 | async-start | bytes 1048576 | tf_op jit(solution)/shard_map/all_to_all | solution.py:34
  266.0 43.4 %all-to-all-start.7 = ((bf16[32,128,32]{1,2,0:T(8,128)(2,1)}), bf16[32,128,32]{1,2,0:T(8,128)(2,1)S(1)}, u32[]{:S(2)}, u32[]{:S(2)}) async-start(bf16[32,128,32]{1,2,0:T(8,128)(2,1)} %broadcast_in_dim.14), calls=%async_computation.7 | async-start | bytes 524288 | tf_op jit(solution)/shard_map/all_to_all | solution.py:20
  310.2 13.4 %all-to-all-start.8 = ((bf16[8,128,8]{1,2,0:T(8,128)(2,1)}), bf16[8,128,8]{1,2,0:T(8,128)(2,1)S(1)}, u32[]{:S(2)}, u32[]{:S(2)}) async-start(bf16[8,128,8]{1,2,0:T(8,128)(2,1)} %fusion.1), calls=%async_computation.8 | async-start | bytes 32768 | tf_op jit(solution)/shard_map/all_to_all | solution.py:51
where the time goes:
time: 325 us; the launch traced here: 324 us
  waiting for transfers between devices  187 us (58%)
  starting transfers between devices  79.9 us (25%)
  blocking collectives  37.3 us (11%)
  local copies, waits for them, and re-layouts  11.9 us (4%)
  matrix products  4.48 us (1%)
    all_to_all x2, waiting for transfers between devices, sent_and_summed(): lax.all_to_all(parts, axis, split_axis=0, concat_axis=0, tiled=True)  119 us
    all_to_all x4, waiting for transfers between devices, from_everyone(): return lax.all_to_all(copies, axis, split_axis=0, concat_axis=0, tiled=True)  64.7 us
    all_to_all x4, starting transfers between devices, from_everyone(): return lax.all_to_all(copies, axis, split_axis=0, concat_axis=0, tiled=True)  59.5 us
    all_to_all x1, blocking collectives, from_everyone(): return lax.all_to_all(copies, axis, split_axis=0, concat_axis=0, tiled=True)  26.7 us
    all_to_all x2, starting transfers between devices, sent_and_summed(): lax.all_to_all(parts, axis, split_axis=0, concat_axis=0, tiled=True)  11.7 us
    all_to_all x1, blocking collectives, summed_on_arrival(): lax.all_to_all(parts, axis, split_axis=0, concat_axis=0, tiled=True)  10.6 us
    all_to_all x1, starting transfers between devices, summed_on_arrival(): lax.all_to_all(parts, axis, split_axis=0, concat_axis=0, tiled=True)  8.68 us
  transfers between devices with their start and end apart: 7, of which 7 were waited for; matrix products, arithmetic and copies ran while one was open for 1% of the time, Pallas kernels for 0%

commit v1 on v0

v1 whole, which is shorter than its diff:
```python
import functools

import jax
import jax.numpy as jnp
from jax import lax
from jax.experimental import pallas as pl
from jax.experimental.pallas import tpu as pltpu
from jax.sharding import PartitionSpec as P

MESH = pl.DeviceIdType.MESH
epsilon = 1e-06
f32 = jnp.float32
bf16 = jnp.bfloat16


def nn(a, b):
    return jnp.dot(a, b, preferred_element_type=f32)


def nt(a, b):
    return lax.dot_general(a, b, (((1,), (1,)), ((), ())), preferred_element_type=f32)


def exact_nn(a, onehot):
    high = a.astype(bf16)
    low = (a - high.astype(f32)).astype(bf16)
    return nn(high, onehot) + nn(low, onehot)


def lanes_of(x, lane):
    at = lax.broadcasted_iota(jnp.int32, x.shape, 1)
    return jnp.sum(jnp.where(at == lane, x, 0.0), axis=1, keepdims=True)


def column_of(row):
    n = row.shape[1]
    eye = lax.broadcasted_iota(jnp.int32, (n, n), 0) == lax.broadcasted_iota(
        jnp.int32, (n, n), 1
    )
    return jnp.sum(jnp.where(eye, row, 0.0), axis=1, keepdims=True)


class Exchange:
    def __init__(self, n_kv, g, z, t):
        self.n_kv, self.g, self.z, self.t = n_kv, g, z, t
        self.half = n_kv // 8
        up = [2 + 4 * i for i in range(self.half)]
        self.reach = up + [-u for u in up]
        self.count = 2 * self.half
        self.steps = [(0, 1), (1, -1)]
        self.farthest_first = [
            k * self.half + i for i in reversed(range(self.half)) for k in (0, 1)
        ]
        self.nearest_first = list(reversed(self.farthest_first))

    def device(self, offset):
        return (self.g, lax.rem(self.z + offset + self.n_kv, self.n_kv), self.t)

    def near(self, i):
        last = () if i == self.count - 1 else ((3, 2 if i < self.half else -2),)
        return self.steps + list(last)

    def copy(self, src, dst, send, recv, offset):
        return pltpu.make_async_remote_copy(
            src_ref=src,
            dst_ref=dst,
            send_sem=send,
            recv_sem=recv,
            device_id=self.device(offset),
            device_id_type=MESH,
        )


def placing(per_slot, n_kv, seq, z):
    count = n_kv // 4
    half = count // 2
    shape = (n_kv * per_slot, n_kv * seq)
    m = lax.broadcasted_iota(jnp.int32, shape, 0)
    slot = m // per_slot
    i = slot % count
    group = slot // count
    reach = jnp.where(i < half, 2 + 4 * i, 4 * half - 2 - 4 * i)
    side = jnp.where(i < half, 2, -2)
    step = jnp.where(group == 0, 1, jnp.where(group == 1, -1, jnp.where(group == 2, 0, side)))
    offset = jnp.where(slot == n_kv - 1, 0, reach + step)
    owner = (z - offset + n_kv) % n_kv
    row = owner * seq + m % seq
    return (row == lax.broadcasted_iota(jnp.int32, shape, 1)).astype(bf16)


def kernel(
    dims,
    tok_ref,
    state_hbm,
    gain_ref,
    wq_hbm,
    wk_hbm,
    wv_hbm,
    wb_hbm,
    wd_hbm,
    alog_ref,
    dt_ref,
    hgain_ref,
    wo_hbm,
    mgain_ref,
    wu_hbm,
    wdn_hbm,
    out_ref,
    state_out,
    tok_all,
    state_v,
    rhs1,
    wext,
    wo_v,
    wu_v,
    wdn_v,
    rs1,
    rs1_near,
    rs1_far_src,
    rs1_far,
    ag2,
    att,
    mid,
    rs3,
    rs3_near,
    rs3_far_src,
    rs3_far,
    sq_src,
    sq_near,
    sq_far_src,
    sq_far,
    ag4,
    low_src,
    low,
    loc,
    tok_s,
    tok_r,
    rs1_ns,
    rs1_nr,
    rs1_fs,
    rs1_fr,
    ag2_ns,
    ag2_nr,
    ag2_fs,
    ag2_fr,
    att_s,
    att_r,
    rs3_ns,
    rs3_nr,
    rs3_fs,
    rs3_fr,
    sq_ns,
    sq_nr,
    sq_fs,
    sq_fr,
    ag4_ns,
    ag4_nr,
    ag4_fs,
    ag4_fr,
    low_s,
    low_r,
    sem_a,
    sem_b,
    sem_c,
):
    n_kv, n_tp, seq, heads, width = dims
    g, z, t = lax.axis_index("grp"), lax.axis_index("kv"), lax.axis_index("tp")
    ex = Exchange(n_kv, g, z, t)
    count, half = ex.count, ex.half
    block = tok_all.shape[0] * tok_all.shape[1]
    mine = tok_all.shape[1]
    head = hgain_ref.shape[1]
    own = n_kv - 1

    def tp_peer(k):
        return (g, z, lax.rem(t + k, n_tp))

    barrier = pltpu.get_barrier_semaphore()
    for k in range(1, n_tp):
        pl.semaphore_signal(barrier, inc=1, device_id=tp_peer(k), device_id_type=MESH)
    for offset in (1, -1, 2, -2):
        pl.semaphore_signal(barrier, inc=1, device_id=ex.device(offset), device_id_type=MESH)

    local = []

    def fetch(src, dst):
        copy = pltpu.make_async_copy(src, dst, loc.at[len(local)])
        copy.start()
        local.append(copy)

    for i, w in enumerate((wq_hbm, wk_hbm)):
        for h in range(heads):
            at = (i * heads + h) * block
            fetch(w.at[:, h * head : (h + 1) * head], rhs1.at[at : at + block, 0:head])
    for h in range(heads):
        fetch(
            wv_hbm.at[:, h * head : (h + 1) * head],
            rhs1.at[h * block : (h + 1) * block, head : 2 * head],
        )
    lanes = wext.shape[2]
    at = pl.multiple_of((z * block // lanes) * lanes, lanes)
    fetch(wb_hbm.at[:, pl.ds(at, lanes)], wext.at[0])
    fetch(wd_hbm.at[:, pl.ds(at, lanes)], wext.at[1])
    first_fetch = len(local)
    fetch(state_hbm, state_v)
    second_fetch = len(local)
    for h in range(heads):
        fetch(wo_hbm.at[:, h * head : (h + 1) * head], wo_v.at[h * block : (h + 1) * block])
    third_fetch = len(local)
    parts = wu_v.shape[0] // block
    wide = wu_v.shape[1]
    for j in range(parts):
        fetch(wu_hbm.at[:, j * wide : (j + 1) * wide], wu_v.at[j * block : (j + 1) * block])
    for j in range(parts):
        fetch(wdn_hbm.at[:, j * wide : (j + 1) * wide], wdn_v.at[j * block : (j + 1) * block])
    all_fetch = len(local)

    tok_all[t] = tok_ref[...].astype(f32)
    rhs1[heads * block :, head:] = jnp.zeros((heads * block, head), bf16)
    spread16 = placing(parts * seq, n_kv, seq, z)
    part_of_row = (
        lax.broadcasted_iota(jnp.int32, (n_kv * parts * seq, parts * block), 0) // seq
    ) % parts
    part_mask = part_of_row == (
        lax.broadcasted_iota(jnp.int32, (n_kv * parts * seq, parts * block), 1) // block
    )
    gain = column_of(gain_ref[...])
    mixer_gain = column_of(mgain_ref[...])

    pl.semaphore_wait(barrier, n_tp - 1 + 4)
    for offset in (2, -2):
        pl.semaphore_signal(sem_a, inc=1, device_id=ex.device(offset), device_id_type=MESH)

    def to_tp(src_of, dst, send, recv):
        copies = []
        for k in range(1, n_tp):
            peer = lax.rem(t + k, n_tp)
            copy = pltpu.make_async_remote_copy(
                src_ref=src_of(peer),
                dst_ref=dst.at[t],
                send_sem=send.at[k - 1],
                recv_sem=recv.at[k - 1],
                device_id=(g, z, peer),
                device_id_type=MESH,
            )
            copy.start()
            copies.append(copy)
        return copies

    pending = []
    copies = to_tp(lambda peer: tok_all.at[t], tok_all, tok_s, tok_r)
    pending += copies
    for k in range(first_fetch):
        local[k].wait()
    odd = lax.rem(z, lanes // block) if lanes // block > 1 else 0
    pieces = []
    for i in range(2):
        piece = wext[i][:, 0:block]
        for k in range(1, lanes // block):
            piece = jnp.where(odd == k, wext[i][:, k * block : (k + 1) * block], piece)
        pieces.append(piece)
    n_heads = pieces[0].shape[0]
    wext_t = jnp.concatenate(
        pieces + [jnp.zeros((head - 2 * n_heads, block), bf16)], axis=0
    )
    at_row = lax.broadcasted_iota(jnp.int32, (head, block), 0)
    square_t = (at_row == 2 * n_heads).astype(bf16)
    ext_t = jnp.concatenate([wext_t, square_t], axis=1)

    pl.semaphore_wait(sem_a, 2)
    for offset in (4, -4):
        pl.semaphore_signal(sem_b, inc=1, device_id=ex.device(offset), device_id_type=MESH)
    for copy in copies:
        copy.wait_recv()

    def spread(x_t):
        stacked = jnp.concatenate([x_t] * parts, axis=0)
        rows = nt(spread16, stacked)
        return jnp.where(part_mask, rows, 0.0).astype(bf16)

    tok_t = tok_all[...].reshape(block, tok_all.shape[2])
    scaled_t = (tok_t * gain).astype(bf16)
    left = spread(scaled_t)
    both = jnp.concatenate([scaled_t, (tok_t * tok_t).astype(bf16)], axis=0)
    left2 = nt(spread16, both)
    left2 = jnp.where(part_of_row[:, 0 : 2 * block] >= heads, left2, 0.0).astype(bf16)
    product = nn(left, rhs1[...])
    extra = nt(left2, ext_t)
    product = jnp.concatenate([product[:, :head], product[:, head:] + extra], axis=1)
    rs1[...] = product.astype(bf16).reshape(rs1.shape)

    def reduce_near(buf, near_buf, send, recv, order):
        started = {}
        for i in order:
            for group, step in ex.near(i):
                k = group * count + i if group < 2 else 2 * count + i
                copy = ex.copy(
                    buf.at[group * count + i],
                    near_buf.at[k],
                    send.at[k],
                    recv.at[k],
                    -step,
                )
                copy.start()
                started[k] = copy
        return started

    def near_sum(i, buf, near_buf, started):
        total = buf[2 * count + i].astype(f32)
        for group, step in ex.near(i):
            k = group * count + i if group < 2 else 2 * count + i
            started[k].wait_recv()
            total += near_buf[k].astype(f32)
        return total

    def reduce_far(i, total, far_src, far_buf, send, recv):
        far_src[i] = total.astype(far_src.dtype)
        copy = ex.copy(far_src.at[i], far_buf.at[i], send.at[i], recv.at[i], -ex.reach[i])
        copy.start()
        return copy

    def far_sum(buf, far_buf, copies):
        total = buf[own].astype(f32)
        for i, copy in copies:
            copy.wait_recv()
            total += far_buf[i].astype(f32)
        return total

    close = [i for i in ex.nearest_first if abs(ex.reach[i]) <= 8]
    distant = [i for i in ex.farthest_first if abs(ex.reach[i]) > 8]
    started = reduce_near(rs1, rs1_near, rs1_ns, rs1_nr, distant + close)
    pending += list(started.values())
    pl.semaphore_wait(sem_b, 2)
    for offset in (8, -8):
        pl.semaphore_signal(sem_c, inc=1, device_id=ex.device(offset), device_id_type=MESH)
    copies = []
    for i in close:
        total = near_sum(i, rs1, rs1_near, started)
        copies.append((i, reduce_far(i, total, rs1_far_src, rs1_far, rs1_fs, rs1_fr)))
    totals = [near_sum(i, rs1, rs1_near, started) for i in distant]
    pl.semaphore_wait(sem_c, 2)
    for i, total in zip(distant, totals):
        copies.append((i, reduce_far(i, total, rs1_far_src, rs1_far, rs1_fs, rs1_fr)))
    pending += [c for _, c in copies]

    local[first_fetch].wait()
    for k in range(second_fetch, third_fetch):
        local[k].wait()
    sums = far_sum(rs1, rs1_far, copies)

    rows = heads * seq
    query_sum, key_sum = sums[:rows, :head], sums[rows:, :head]
    value_sum, extra = sums[:rows, head:], sums[rows:, head:]
    which = lax.broadcasted_iota(jnp.int32, (rows, head), 0) // seq
    lane = lax.broadcasted_iota(jnp.int32, (rows, head), 1)
    beta_sum = jnp.sum(
        jnp.where(lane == t * heads + which, extra, 0.0), axis=1, keepdims=True
    )
    decay_sum = jnp.sum(
        jnp.where(lane == n_heads + t * heads + which, extra, 0.0), axis=1, keepdims=True
    )
    square_sum = lanes_of(extra, 2 * n_heads)
    first = lax.rsqrt(square_sum / width + epsilon)
    query_pre, key_pre, value_pre = first * query_sum, first * key_sum, first * value_sum
    query = query_pre * lax.rsqrt(jnp.sum(query_pre * query_pre, axis=1, keepdims=True) + epsilon)
    key = key_pre * lax.rsqrt(jnp.sum(key_pre * key_pre, axis=1, keepdims=True) + epsilon)
    beta = jax.nn.sigmoid(first * beta_sum)
    which1 = lax.broadcasted_iota(jnp.int32, (rows, 1), 0) // seq
    a_log = jnp.zeros((rows, 1), f32)
    dt_bias = jnp.zeros((rows, 1), f32)
    for h in range(heads):
        a_log = jnp.where(which1 == h, alog_ref[h], a_log)
        dt_bias = jnp.where(which1 == h, dt_ref[h], dt_bias)
    logit = first * decay_sum + dt_bias
    softplus = jnp.maximum(logit, 0.0) + jnp.log1p(jnp.exp(-jnp.abs(logit)))
    decay = jnp.exp(-jnp.exp(a_log) * softplus)
    query_t, key_t = query.T, key.T
    key_reads, query_reads = [], []
    for k in range(rows):
        matrix = state_v[k % seq, k // seq]
        key_reads.append(jnp.sum(matrix * key_t[:, k : k + 1], axis=0, keepdims=True))
        query_reads.append(jnp.sum(matrix * query_t[:, k : k + 1], axis=0, keepdims=True))
    key_read = jnp.concatenate(key_reads, axis=0)
    query_read = jnp.concatenate(query_reads, axis=0)
    fresh = beta * (value_pre - decay * key_read)
    meeting = jnp.sum(query * key, axis=1, keepdims=True)
    reading = decay * query_read + meeting * fresh
    normed = (
        reading
        * lax.rsqrt(jnp.mean(reading * reading, axis=1, keepdims=True) + epsilon)
        * hgain_ref[...]
    )

    def gather_far(buf, send, recv):
        copies = {}
        for i in ex.farthest_first:
            copy = ex.copy(
                buf.at[own], buf.at[2 * count + i], send.at[i], recv.at[i], ex.reach[i]
            )
            copy.start()
            copies[i] = copy
        return copies

    def gather_near(buf, copies, send, recv):
        started = []
        for i in ex.nearest_first:
            copies[i].wait_recv()
            for group, step in ex.near(i):
                k = group * count + i if group < 2 else 2 * count + i
                copy = ex.copy(
                    buf.at[2 * count + i],
                    buf.at[group * count + i],
                    send.at[k],
                    recv.at[k],
                    step,
                )
                copy.start()
                started.append(copy)
        return started

    ag2[own] = normed.astype(bf16).astype(f32)
    copies = gather_far(ag2, ag2_fs, ag2_fr)
    pending += list(copies.values())
    for k in range(rows):
        matrix = state_v[k % seq, k // seq]
        state_v[k % seq, k // seq] = (
            decay[k : k + 1] * matrix + key_t[:, k : k + 1] * fresh[k : k + 1]
        )
    store = pltpu.make_async_copy(state_v, state_out, loc.at[all_fetch])
    store.start()
    spread8 = placing(heads * seq, n_kv, seq, z)
    head_of_column = (
        lax.broadcasted_iota(jnp.int32, (block, n_kv * rows), 1) // seq
    ) % heads
    started = gather_near(ag2, copies, ag2_ns, ag2_nr)
    pending += started
    for copy in started:
        copy.wait_recv()
    everyone = ag2[...].reshape(n_kv * rows, head).astype(bf16)
    by_head = nt(wo_v[...], everyone)
    chosen = by_head[0:block]
    for h in range(1, heads):
        chosen = jnp.where(head_of_column == h, by_head[h * block : (h + 1) * block], chosen)
    att[t] = exact_nn(chosen, spread8).astype(bf16)
    copies = to_tp(lambda peer: att.at[t], att, att_s, att_r)
    pending += copies
    for k in range(third_fetch, all_fetch):
        local[k].wait()
    for copy in copies:
        copy.wait_recv()
    attended = att[0].astype(f32)
    for k in range(1, n_tp):
        attended += att[k].astype(f32)
    middle = (tok_t + attended).astype(bf16).astype(f32)
    mid[...] = middle.reshape(mid.shape)

    scaled_t = (middle * mixer_gain).astype(bf16)
    left = spread(scaled_t)
    rs3[...] = nn(left, wu_v[...]).astype(bf16).reshape(rs3.shape)
    started = reduce_near(rs3, rs3_near, rs3_ns, rs3_nr, ex.farthest_first)
    pending += list(started.values())
    square_part = jnp.sum(middle * middle, axis=0, keepdims=True)
    sq_src[...] = square_part
    sq_started = []
    for k, step in enumerate((1, -1, 2, -2)):
        copy = ex.copy(sq_src, sq_near.at[k], sq_ns.at[k], sq_nr.at[k], -step)
        copy.start()
        sq_started.append(copy)
    pending += sq_started
    copies = []
    for i in ex.farthest_first:
        total = near_sum(i, rs3, rs3_near, started)
        copies.append((i, reduce_far(i, total, rs3_far_src, rs3_far, rs3_fs, rs3_fr)))
    pending += [c for _, c in copies]
    for copy in sq_started:
        copy.wait_recv()
    base = square_part + sq_near[0] + sq_near[1]
    sq_far_src[0] = base + sq_near[2]
    sq_far_src[1] = base + sq_near[3]
    sq_far_src[2] = base
    sq_copies = []
    for i in ex.farthest_first:
        which_sum = 2 if i == count - 1 else (0 if i < half else 1)
        copy = ex.copy(
            sq_far_src.at[which_sum], sq_far.at[i], sq_fs.at[i], sq_fr.at[i], -ex.reach[i]
        )
        copy.start()
        sq_copies.append(copy)
    pending += sq_copies
    for copy in sq_copies:
        copy.wait_recv()
    square_two = square_part
    for i in range(count):
        square_two += sq_far[i]
    second_all = lax.rsqrt(square_two / width + epsilon)
    row_of = z * seq + lax.broadcasted_iota(
        jnp.int32, (parts * seq, second_all.shape[1]), 0
    ) % seq
    lane_of = lax.broadcasted_iota(jnp.int32, (parts * seq, second_all.shape[1]), 1)
    second = jnp.sum(jnp.where(lane_of == row_of, second_all, 0.0), axis=1, keepdims=True)
    up = far_sum(rs3, rs3_far, copies)
    hidden = jnp.square(jnp.maximum(second * up, 0.0)).astype(bf16)

    ag4[own] = hidden
    copies = gather_far(ag4, ag4_fs, ag4_fr)
    pending += list(copies.values())
    started = gather_near(ag4, copies, ag4_ns, ag4_nr)
    pending += started
    for copy in started:
        copy.wait_recv()
    everyone = ag4[...].reshape(n_kv * parts * seq, wide)
    by_part = nt(wdn_v[...], everyone)
    part_of_column = (
        lax.broadcasted_iota(jnp.int32, (block, n_kv * parts * seq), 1) // seq
    ) % parts
    chosen = by_part[0:block]
    for j in range(1, parts):
        chosen = jnp.where(part_of_column == j, by_part[j * block : (j + 1) * block], chosen)
    lowered_part = exact_nn(chosen, spread16).astype(bf16).astype(f32)
    low_src[...] = lowered_part.reshape(low_src.shape)
    copies = to_tp(lambda peer: low_src.at[peer], low, low_s, low_r)
    pending += copies
    low[t] = low_src[t]
    for copy in copies:
        copy.wait_recv()
    lowered = low[0]
    for k in range(1, n_tp):
        lowered += low[k]
    out_ref[...] = (mid[t] + lowered).astype(bf16)
    for copy in pending:
        copy.wait_send()
    store.wait()


def solution(mesh):
    n_kv, n_tp = mesh.shape["kv"], mesh.shape["tp"]

    def local(
        tokens,
        state,
        norm_gain,
        w_query,
        w_key,
        w_value,
        w_beta,
        w_decay,
        a_log,
        dt_bias,
        head_gain,
        w_out,
        mixer_gain,
        w_up,
        w_down,
    ):
        seq, heads, head = state.shape[:3]
        rows, mine = tokens.shape
        block = w_query.shape[0]
        parts = w_up.shape[1] * seq * n_kv // (rows * 2 * head)
        wide = w_up.shape[1] // parts
        count = n_kv // 4
        dims = (n_kv, n_tp, seq, heads, block * n_kv)
        vmem, hbm, smem = (
            pl.BlockSpec(memory_space=pltpu.VMEM),
            pl.BlockSpec(memory_space=pl.ANY),
            pl.BlockSpec(memory_space=pltpu.SMEM),
        )
        dma = pltpu.SemaphoreType.DMA
        blocks = (parts * seq, wide)
        near = (3 * count - 1,)
        n_local = 3 * heads + 2 + 1 + heads + 2 * parts + 1
        scratch = [
            pltpu.VMEM((n_tp, mine, rows), f32),
            pltpu.VMEM(state.shape, f32),
            pltpu.VMEM((2 * heads * block, 2 * head), bf16),
            pltpu.VMEM((2, w_beta.shape[1], head), bf16),
            pltpu.VMEM((heads * block, head), bf16),
            pltpu.VMEM((parts * block, wide), bf16),
            pltpu.VMEM((parts * block, wide), bf16),
            pltpu.VMEM((n_kv, *blocks), bf16),
            pltpu.VMEM((3 * count - 1, *blocks), bf16),
            pltpu.VMEM((count, *blocks), bf16),
            pltpu.VMEM((count, *blocks), bf16),
            pltpu.VMEM((n_kv, heads * seq, head), f32),
            pltpu.VMEM((n_tp, block, rows), bf16),
            pltpu.VMEM((n_tp, mine, rows), f32),
            pltpu.VMEM((n_kv, *blocks), bf16),
            pltpu.VMEM((3 * count - 1, *blocks), bf16),
            pltpu.VMEM((count, *blocks), bf16),
            pltpu.VMEM((count, *blocks), bf16),
            pltpu.VMEM((1, rows), f32),
            pltpu.VMEM((4, 1, rows), f32),
            pltpu.VMEM((3, 1, rows), f32),
            pltpu.VMEM((count, 1, rows), f32),
            pltpu.VMEM((n_kv, *blocks), bf16),
            pltpu.VMEM((n_tp, mine, rows), f32),
            pltpu.VMEM((n_tp, mine, rows), f32),
            dma((n_local,)),
            dma((n_tp - 1,)),
            dma((n_tp - 1,)),
            dma(near),
            dma(near),
            dma((count,)),
            dma((count,)),
            dma(near),
            dma(near),
            dma((count,)),
            dma((count,)),
            dma((n_tp - 1,)),
            dma((n_tp - 1,)),
            dma(near),
            dma(near),
            dma((count,)),
            dma((count,)),
            dma((4,)),
            dma((4,)),
            dma((count,)),
            dma((count,)),
            dma(near),
            dma(near),
            dma((count,)),
            dma((count,)),
            dma((n_tp - 1,)),
            dma((n_tp - 1,)),
            pltpu.SemaphoreType.REGULAR,
            pltpu.SemaphoreType.REGULAR,
            pltpu.SemaphoreType.REGULAR,
        ]
        mixed_t, new_state = pl.pallas_call(
            functools.partial(kernel, dims),
            out_shape=(
                jax.ShapeDtypeStruct((mine, rows), bf16),
                jax.ShapeDtypeStruct(state.shape, f32),
            ),
            in_specs=[
                vmem,
                hbm,
                vmem,
                hbm,
                hbm,
                hbm,
                hbm,
                hbm,
                smem,
                smem,
                vmem,
                hbm,
                vmem,
                hbm,
                hbm,
            ],
            out_specs=(vmem, hbm),
            scratch_shapes=scratch,
            compiler_params=pltpu.CompilerParams(collective_id=0, has_side_effects=True),
        )(
            tokens.T,
            state,
            norm_gain.astype(f32).reshape(1, block),
            w_query,
            w_key,
            w_value,
            w_beta.T,
            w_decay.T,
            a_log,
            dt_bias,
            head_gain.reshape(1, head),
            w_out.T,
            mixer_gain.astype(f32).reshape(1, block),
            w_up,
            w_down.T,
        )
        return mixed_t.T, new_state

    return jax.shard_map(
        local,
        mesh=mesh,
        in_specs=(
            P("grp", ("kv", "tp")),
            P(("grp", "kv"), "tp", None, None),
            P("kv"),
            P("kv", "tp"),
            P("kv", "tp"),
            P("kv", "tp"),
            P(),
            P(),
            P("tp"),
            P("tp"),
            P(),
            P("tp", "kv"),
            P("kv"),
            P("kv", "tp"),
            P("tp", "kv"),
        ),
        out_specs=(P("grp", ("kv", "tp")), P(("grp", "kv"), "tp", None, None)),
        check_vma=False,
    )
```

time: 325 us -> 135 us (0.42)
  waiting for transfers between devices: 187 us -> 0 us
  Pallas kernels: 0 us -> 130 us
  starting transfers between devices: 79.9 us -> 0 us
  blocking collectives: 37.3 us -> 0 us
  local copies, waits for them, and re-layouts: 11.9 us -> 3.77 us
  matrix products: 4.48 us -> 0 us
    all_to_all x7 -> x0, waiting for transfers between devices: 187 us -> none  [the longest x2 119 us: sent_and_summed(): lax.all_to_all(parts, axis, split_axis=0, concat_axis=0, tiled=True)]
    pallas_call x0 -> x1, Pallas kernels: none -> 130 us  [local(): pl.pallas_call(functools.partial(kernel, dims), out_shape=(jax.ShapeDtype...]
    all_to_all x7 -> x0, starting transfers between devices: 79.9 us -> none  [the longest x4 59.5 us: from_everyone(): return lax.all_to_all(copies, axis, split_axis=0, concat_axis=0, tiled=True)]
    all_to_all x2 -> x0, blocking collectives: 37.3 us -> none  [the longest x1 26.7 us: from_everyone(): return lax.all_to_all(copies, axis, split_axis=0, concat_axis=0, tiled=True)]
    dot_general x10 -> x0, matrix products: 4.48 us -> none  [the longest x8 4.11 us: dotted(): return jnp.dot(left, right, preferred_element_type=jnp.float32)]
    broadcast_in_dim x5 -> x0, local copies, waits for them, and re-layouts: 3.3 us -> none  [from_everyone(): copies = jnp.broadcast_to(x, (lax.axis_size(axis), *x.shape))]
  transfers between devices with their start and end apart: 7 -> 0, of which waited for: 7 -> 0; matrix products, arithmetic and copies ran while one was open for 1% -> 0% of each run, Pallas kernels for 0% -> 0%
where the time goes in v1:
time: 135 us
  Pallas kernels  130 us (96%)
  local copies, waits for them, and re-layouts  3.77 us (3%)
    pallas_call x1, Pallas kernels, local(): pl.pallas_call(functools.partial(kernel, dims), out_shape=(jax.ShapeDtype...  130 us
    unnamed x8, local copies, waits for them, and re-layouts  3.77 us

profile of v1, /device:TPU:33, one launch (start us, length us, event | category | flops | bytes accessed | tf_op | source)
XLA Modules:
  0.0 134.6 jit_solution(13886803009723589617)
XLA Ops:
  0.6 0.0 copy-start.1
  0.6 0.0 copy-start.2
  0.6 0.6 copy-done.1
  1.3 0.0 copy-done.2
  1.3 0.5 bitcast_convert_fusion
  1.8 129.6 %shard_map.158 = (bf16[8,128]{1,0:T(8,128)(2,1)}, f32[4,2,128,128]{3,2,1,0:T(8,128)}) custom-call(bf16[8,128]{1,0:T(8,128)(2,1)} %bitcast.17, f32[4,2,128,128]{3,2,1,0:T(8,128)} %state_hbm.1, f32[1,64]{1,0:T(1,128)} %get-tuple-element.7.gain_ref, bf16[64,256]{1,0:T(8,128)(2,1)} %wq_hbm.1, bf16[64,256]{1,0:T(8,128)(2,1)} %wk_hbm.1, bf16[64,256]{1,0:T(8,128)(2,1)} %wv_hbm.1, ...), custom_call_target="tpu_custom_call" | custom-call | tf_op jit(solution)/shard_map/pallas_call | solution.py:628
  131.5 0.0 copy-start
  131.5 0.7 copy-done
  132.1 0.6 copy.19
  132.7 1.9 %copy.20 = f32[4,2,128,128]{3,2,1,0:T(8,128)} copy(f32[4,2,128,128]{3,2,1,0:T(8,128)} %get-tuple-element.11) | data formatting | bytes 1048576
Async XLA Ops:
  0.6 0.7 copy-start.1
  0.6 0.7 copy-start.2
  131.5 0.7 copy-start

commit v2 on v1

--- a/solution.py
+++ b/solution.py
@@ -43,22 +43,29 @@
 class Exchange:
     def __init__(self, n_kv, g, z, t):
         self.n_kv, self.g, self.z, self.t = n_kv, g, z, t
-        self.half = n_kv // 8
-        up = [2 + 4 * i for i in range(self.half)]
+        self.half = (n_kv // 2 - 1) // 3
+        up = [3 + 3 * i for i in range(self.half)]
         self.reach = up + [-u for u in up]
         self.count = 2 * self.half
-        self.steps = [(0, 1), (1, -1)]
         self.farthest_first = [
             k * self.half + i for i in reversed(range(self.half)) for k in (0, 1)
         ]
         self.nearest_first = list(reversed(self.farthest_first))
+        self.own = self.middle(self.count)
+
+    def middle(self, i):
+        return self.count + 1 + i
+
+    def near(self, i):
+        n = self.count + 1
+        above = [(i, i, 1)]
+        if i == self.count - 1:
+            return above
+        j = i if i < self.count else i - 1
+        return above + [(2 * n + j, n + j, -1)]
 
     def device(self, offset):
         return (self.g, lax.rem(self.z + offset + self.n_kv, self.n_kv), self.t)
-
-    def near(self, i):
-        last = () if i == self.count - 1 else ((3, 2 if i < self.half else -2),)
-        return self.steps + list(last)
 
     def copy(self, src, dst, send, recv, offset):
         return pltpu.make_async_remote_copy(
@@ -72,18 +79,16 @@
 
 
 def placing(per_slot, n_kv, seq, z):
-    count = n_kv // 4
-    half = count // 2
+    half = (n_kv // 2 - 1) // 3
+    n = 2 * half + 1
     shape = (n_kv * per_slot, n_kv * seq)
     m = lax.broadcasted_iota(jnp.int32, shape, 0)
     slot = m // per_slot
-    i = slot % count
-    group = slot // count
-    reach = jnp.where(i < half, 2 + 4 * i, 4 * half - 2 - 4 * i)
-    side = jnp.where(i < half, 2, -2)
-    step = jnp.where(group == 0, 1, jnp.where(group == 1, -1, jnp.where(group == 2, 0, side)))
-    offset = jnp.where(slot == n_kv - 1, 0, reach + step)
-    owner = (z - offset + n_kv) % n_kv
+    group = (slot >= n).astype(jnp.int32) + (slot >= 2 * n).astype(jnp.int32)
+    i = slot - n * group
+    reach = jnp.where(i < half, 3 + 3 * i, 3 * half - 3 - 3 * i)
+    reach = jnp.where((i == n - 1) | (slot == n_kv - 1), 0, reach)
+    owner = (z - (reach + 1 - group) + n_kv) % n_kv
     row = owner * seq + m % seq
     return (row == lax.broadcasted_iota(jnp.int32, shape, 1)).astype(bf16)
 
@@ -166,11 +171,11 @@
     n_kv, n_tp, seq, heads, width = dims
     g, z, t = lax.axis_index("grp"), lax.axis_index("kv"), lax.axis_index("tp")
     ex = Exchange(n_kv, g, z, t)
-    count, half = ex.count, ex.half
+    count = ex.count
     block = tok_all.shape[0] * tok_all.shape[1]
     mine = tok_all.shape[1]
     head = hgain_ref.shape[1]
-    own = n_kv - 1
+    own = ex.own
 
     def tp_peer(k):
         return (g, z, lax.rem(t + k, n_tp))
@@ -178,7 +183,7 @@
     barrier = pltpu.get_barrier_semaphore()
     for k in range(1, n_tp):
         pl.semaphore_signal(barrier, inc=1, device_id=tp_peer(k), device_id_type=MESH)
-    for offset in (1, -1, 2, -2):
+    for offset in (1, -1, 3, -3):
         pl.semaphore_signal(barrier, inc=1, device_id=ex.device(offset), device_id_type=MESH)
 
     local = []
@@ -228,7 +233,7 @@
     mixer_gain = column_of(mgain_ref[...])
 
     pl.semaphore_wait(barrier, n_tp - 1 + 4)
-    for offset in (2, -2):
+    for offset in (3, -3):
         pl.semaphore_signal(sem_a, inc=1, device_id=ex.device(offset), device_id_type=MESH)
 
     def to_tp(src_of, dst, send, recv):
@@ -268,7 +273,7 @@
     ext_t = jnp.concatenate([wext_t, square_t], axis=1)
 
     pl.semaphore_wait(sem_a, 2)
-    for offset in (4, -4):
+    for offset in (6, -6):
         pl.semaphore_signal(sem_b, inc=1, device_id=ex.device(offset), device_id_type=MESH)
     for copy in copies:
         copy.wait_recv()
@@ -289,26 +294,18 @@
     product = jnp.concatenate([product[:, :head], product[:, head:] + extra], axis=1)
     rs1[...] = product.astype(bf16).reshape(rs1.shape)
 
-    def reduce_near(buf, near_buf, send, recv, order):
+    def reduce_near(buf, near_buf, send, recv):
         started = {}
-        for i in order:
-            for group, step in ex.near(i):
-                k = group * count + i if group < 2 else 2 * count + i
-                copy = ex.copy(
-                    buf.at[group * count + i],
-                    near_buf.at[k],
-                    send.at[k],
-                    recv.at[k],
-                    -step,
-                )
+        for i in ex.farthest_first + [count]:
+            for slot, k, step in ex.near(i):
+                copy = ex.copy(buf.at[slot], near_buf.at[k], send.at[k], recv.at[k], -step)
                 copy.start()
                 started[k] = copy
         return started
 
     def near_sum(i, buf, near_buf, started):
-        total = buf[2 * count + i].astype(f32)
-        for group, step in ex.near(i):
-            k = group * count + i if group < 2 else 2 * count + i
+        total = buf[ex.middle(i)].astype(f32)
+        for _, k, _ in ex.near(i):
             started[k].wait_recv()
             total += near_buf[k].astype(f32)
         return total
@@ -319,34 +316,34 @@
         copy.start()
         return copy
 
-    def far_sum(buf, far_buf, copies):
-        total = buf[own].astype(f32)
-        for i, copy in copies:
+    def far_sum(total, far_buf, copies):
+        for i, copy in reversed(copies):
             copy.wait_recv()
             total += far_buf[i].astype(f32)
         return total
 
-    close = [i for i in ex.nearest_first if abs(ex.reach[i]) <= 8]
-    distant = [i for i in ex.farthest_first if abs(ex.reach[i]) > 8]
-    started = reduce_near(rs1, rs1_near, rs1_ns, rs1_nr, distant + close)
+    started = reduce_near(rs1, rs1_near, rs1_ns, rs1_nr)
     pending += list(started.values())
     pl.semaphore_wait(sem_b, 2)
-    for offset in (8, -8):
+    for offset in (3, -3):
         pl.semaphore_signal(sem_c, inc=1, device_id=ex.device(offset), device_id_type=MESH)
     copies = []
-    for i in close:
-        total = near_sum(i, rs1, rs1_near, started)
-        copies.append((i, reduce_far(i, total, rs1_far_src, rs1_far, rs1_fs, rs1_fr)))
-    totals = [near_sum(i, rs1, rs1_near, started) for i in distant]
+    last = [i for i in ex.farthest_first if abs(ex.reach[i]) > 12]
+    for i in ex.farthest_first:
+        if i not in last:
+            total = near_sum(i, rs1, rs1_near, started)
+            copies.append((i, reduce_far(i, total, rs1_far_src, rs1_far, rs1_fs, rs1_fr)))
+    totals = [near_sum(i, rs1, rs1_near, started) for i in last]
     pl.semaphore_wait(sem_c, 2)
-    for i, total in zip(distant, totals):
-        copies.append((i, reduce_far(i, total, rs1_far_src, rs1_far, rs1_fs, rs1_fr)))
+    for i, total in zip(last, totals):
+        copies.insert(0, (i, reduce_far(i, total, rs1_far_src, rs1_far, rs1_fs, rs1_fr)))
+    home = near_sum(count, rs1, rs1_near, started)
     pending += [c for _, c in copies]
 
     local[first_fetch].wait()
     for k in range(second_fetch, third_fetch):
         local[k].wait()
-    sums = far_sum(rs1, rs1_far, copies)
+    sums = far_sum(home, rs1_far, copies)
 
     rows = heads * seq
     query_sum, key_sum = sums[:rows, :head], sums[rows:, :head]
@@ -391,35 +388,37 @@
         * hgain_ref[...]
     )
 
-    def gather_far(buf, send, recv):
+    def gather_far(buf, far_send, far_recv, send, recv):
         copies = {}
         for i in ex.farthest_first:
             copy = ex.copy(
-                buf.at[own], buf.at[2 * count + i], send.at[i], recv.at[i], ex.reach[i]
+                buf.at[own],
+                buf.at[ex.middle(i)],
+                far_send.at[i],
+                far_recv.at[i],
+                ex.reach[i],
             )
             copy.start()
             copies[i] = copy
-        return copies
+        return copies, pass_on(count, buf, send, recv)
+
+    def pass_on(i, buf, send, recv):
+        started = []
+        for slot, k, step in ex.near(i):
+            copy = ex.copy(buf.at[ex.middle(i)], buf.at[slot], send.at[k], recv.at[k], step)
+            copy.start()
+            started.append(copy)
+        return started
 
     def gather_near(buf, copies, send, recv):
         started = []
         for i in ex.nearest_first:
             copies[i].wait_recv()
-            for group, step in ex.near(i):
-                k = group * count + i if group < 2 else 2 * count + i
-                copy = ex.copy(
-                    buf.at[2 * count + i],
-                    buf.at[group * count + i],
-                    send.at[k],
-                    recv.at[k],
-                    step,
-                )
-                copy.start()
-                started.append(copy)
+            started += pass_on(i, buf, send, recv)
         return started
 
-    ag2[own] = normed.astype(bf16).astype(f32)
-    copies = gather_far(ag2, ag2_fs, ag2_fr)
+    ag2[own] = normed.astype(bf16)
+    copies, started = gather_far(ag2, ag2_fs, ag2_fr, ag2_ns, ag2_nr)
     pending += list(copies.values())
     for k in range(rows):
         matrix = state_v[k % seq, k // seq]
@@ -432,11 +431,11 @@
     head_of_column = (
         lax.broadcasted_iota(jnp.int32, (block, n_kv * rows), 1) // seq
     ) % heads
-    started = gather_near(ag2, copies, ag2_ns, ag2_nr)
+    started += gather_near(ag2, copies, ag2_ns, ag2_nr)
     pending += started
     for copy in started:
         copy.wait_recv()
-    everyone = ag2[...].reshape(n_kv * rows, head).astype(bf16)
+    everyone = ag2[...].astype(f32).reshape(n_kv * rows, head).astype(bf16)
     by_head = nt(wo_v[...], everyone)
     chosen = by_head[0:block]
     for h in range(1, heads):
@@ -457,12 +456,12 @@
     scaled_t = (middle * mixer_gain).astype(bf16)
     left = spread(scaled_t)
     rs3[...] = nn(left, wu_v[...]).astype(bf16).reshape(rs3.shape)
-    started = reduce_near(rs3, rs3_near, rs3_ns, rs3_nr, ex.farthest_first)
+    started = reduce_near(rs3, rs3_near, rs3_ns, rs3_nr)
     pending += list(started.values())
     square_part = jnp.sum(middle * middle, axis=0, keepdims=True)
     sq_src[...] = square_part
     sq_started = []
-    for k, step in enumerate((1, -1, 2, -2)):
+    for k, step in enumerate((1, -1)):
         copy = ex.copy(sq_src, sq_near.at[k], sq_ns.at[k], sq_nr.at[k], -step)
         copy.start()
         sq_started.append(copy)
@@ -474,22 +473,25 @@
     pending += [c for _, c in copies]
     for copy in sq_started:
         copy.wait_recv()
-    base = square_part + sq_near[0] + sq_near[1]
-    sq_far_src[0] = base + sq_near[2]
-    sq_far_src[1] = base + sq_near[3]
-    sq_far_src[2] = base
+    above = square_part + sq_near[0]
+    square_two = above + sq_near[1]
+    sq_far_src[0] = square_two
+    sq_far_src[1] = above
     sq_copies = []
     for i in ex.farthest_first:
-        which_sum = 2 if i == count - 1 else (0 if i < half else 1)
         copy = ex.copy(
-            sq_far_src.at[which_sum], sq_far.at[i], sq_fs.at[i], sq_fr.at[i], -ex.reach[i]
+            sq_far_src.at[int(i == count - 1)],
+            sq_far.at[i],
+            sq_fs.at[i],
+            sq_fr.at[i],
+            -ex.reach[i],
         )
         copy.start()
         sq_copies.append(copy)
     pending += sq_copies
+    home = near_sum(count, rs3, rs3_near, started)
     for copy in sq_copies:
         copy.wait_recv()
-    square_two = square_part
     for i in range(count):
         square_two += sq_far[i]
     second_all = lax.rsqrt(square_two / width + epsilon)
@@ -498,13 +500,13 @@
     ) % seq
     lane_of = lax.broadcasted_iota(jnp.int32, (parts * seq, second_all.shape[1]), 1)
     second = jnp.sum(jnp.where(lane_of == row_of, second_all, 0.0), axis=1, keepdims=True)
-    up = far_sum(rs3, rs3_far, copies)
+    up = far_sum(home, rs3_far, copies)
     hidden = jnp.square(jnp.maximum(second * up, 0.0)).astype(bf16)
 
     ag4[own] = hidden
-    copies = gather_far(ag4, ag4_fs, ag4_fr)
+    copies, started = gather_far(ag4, ag4_fs, ag4_fr, ag4_ns, ag4_nr)
     pending += list(copies.values())
-    started = gather_near(ag4, copies, ag4_ns, ag4_nr)
+    started += gather_near(ag4, copies, ag4_ns, ag4_nr)
     pending += started
     for copy in started:
         copy.wait_recv()
@@ -555,9 +557,9 @@
         seq, heads, head = state.shape[:3]
         rows, mine = tokens.shape
         block = w_query.shape[0]
-        parts = w_up.shape[1] * seq * n_kv // (rows * 2 * head)
+        parts = w_up.shape[1] // (2 * head)
         wide = w_up.shape[1] // parts
-        count = n_kv // 4
+        count = 2 * ((n_kv // 2 - 1) // 3)
         dims = (n_kv, n_tp, seq, heads, block * n_kv)
         vmem, hbm, smem = (
             pl.BlockSpec(memory_space=pltpu.VMEM),
@@ -566,7 +568,7 @@
         )
         dma = pltpu.SemaphoreType.DMA
         blocks = (parts * seq, wide)
-        near = (3 * count - 1,)
+        near = (n_kv - count - 1,)
         n_local = 3 * heads + 2 + 1 + heads + 2 * parts + 1
         scratch = [
             pltpu.VMEM((n_tp, mine, rows), f32),
@@ -577,19 +579,19 @@
             pltpu.VMEM((parts * block, wide), bf16),
             pltpu.VMEM((parts * block, wide), bf16),
             pltpu.VMEM((n_kv, *blocks), bf16),
-            pltpu.VMEM((3 * count - 1, *blocks), bf16),
+            pltpu.VMEM((*near, *blocks), bf16),
             pltpu.VMEM((count, *blocks), bf16),
             pltpu.VMEM((count, *blocks), bf16),
-            pltpu.VMEM((n_kv, heads * seq, head), f32),
+            pltpu.VMEM((n_kv, heads * seq, head), bf16),
             pltpu.VMEM((n_tp, block, rows), bf16),
             pltpu.VMEM((n_tp, mine, rows), f32),
             pltpu.VMEM((n_kv, *blocks), bf16),
-            pltpu.VMEM((3 * count - 1, *blocks), bf16),
+            pltpu.VMEM((*near, *blocks), bf16),
             pltpu.VMEM((count, *blocks), bf16),
             pltpu.VMEM((count, *blocks), bf16),
             pltpu.VMEM((1, rows), f32),
-            pltpu.VMEM((4, 1, rows), f32),
-            pltpu.VMEM((3, 1, rows), f32),
+            pltpu.VMEM((2, 1, rows), f32),
+            pltpu.VMEM((2, 1, rows), f32),
             pltpu.VMEM((count, 1, rows), f32),
             pltpu.VMEM((n_kv, *blocks), bf16),
             pltpu.VMEM((n_tp, mine, rows), f32),
@@ -611,8 +613,8 @@
             dma(near),
             dma((count,)),
             dma((count,)),
-            dma((4,)),
-            dma((4,)),
+            dma((2,)),
+            dma((2,)),
             dma((count,)),
             dma((count,)),
             dma(near),

time: 135 us -> 145 us (1.074)
  Pallas kernels: 130 us -> 140 us
    pallas_call x1, Pallas kernels: 130 us -> 140 us  [local(): pl.pallas_call(functools.partial(kernel, dims), out_shape=(jax.ShapeDtype...]
where the time goes in v2:
time: 145 us
  Pallas kernels  140 us (97%)
  local copies, waits for them, and re-layouts  3.77 us (3%)
    pallas_call x1, Pallas kernels, local(): pl.pallas_call(functools.partial(kernel, dims), out_shape=(jax.ShapeDtype...  140 us
    unnamed x8, local copies, waits for them, and re-layouts  3.77 us

profile of v2, /device:TPU:33, one launch (start us, length us, event | category | flops | bytes accessed | tf_op | source)
XLA Modules:
  0.0 144.9 jit_solution(5817664735965427052)
XLA Ops:
  0.6 0.0 copy-start.1
  0.6 0.0 copy-start.2
  0.6 0.6 copy-done.1
  1.3 0.0 copy-done.2
  1.3 0.5 bitcast_convert_fusion
  1.8 140.0 %shard_map.158 = (bf16[8,128]{1,0:T(8,128)(2,1)}, f32[4,2,128,128]{3,2,1,0:T(8,128)}) custom-call(bf16[8,128]{1,0:T(8,128)(2,1)} %bitcast.17, f32[4,2,128,128]{3,2,1,0:T(8,128)} %state_hbm.1, f32[1,64]{1,0:T(1,128)} %get-tuple-element.7.gain_ref, bf16[64,256]{1,0:T(8,128)(2,1)} %wq_hbm.1, bf16[64,256]{1,0:T(8,128)(2,1)} %wk_hbm.1, bf16[64,256]{1,0:T(8,128)(2,1)} %wv_hbm.1, ...), custom_call_target="tpu_custom_call" | custom-call | tf_op jit(solution)/shard_map/pallas_call | solution.py:630
  141.8 0.0 copy-start
  141.8 0.7 copy-done
  142.5 0.6 copy.19
  143.0 1.9 %copy.20 = f32[4,2,128,128]{3,2,1,0:T(8,128)} copy(f32[4,2,128,128]{3,2,1,0:T(8,128)} %get-tuple-element.11) | data formatting | bytes 1048576
Async XLA Ops:
  0.6 0.7 copy-start.1
  0.6 0.7 copy-start.2
  141.8 0.7 copy-start

commit v3 on v1

--- a/solution.py
+++ b/solution.py
@@ -38,6 +38,10 @@
         jnp.int32, (n, n), 1
     )
     return jnp.sum(jnp.where(eye, row, 0.0), axis=1, keepdims=True)
+
+
+UP_WINDOW = (-1, 0, 1, 2)
+DOWN_WINDOW = (-2, -1, 0, 1)
 
 
 class Exchange:
@@ -108,6 +112,7 @@
     out_ref,
     state_out,
     tok_all,
+    tok_near,
     state_v,
     rhs1,
     wext,
@@ -118,20 +123,20 @@
     rs1_near,
     rs1_far_src,
     rs1_far,
+    ag2_src,
     ag2,
+    diag,
     att,
+    mid_src,
     mid,
     rs3,
-    rs3_near,
-    rs3_far_src,
     rs3_far,
     sq_src,
-    sq_near,
-    sq_far_src,
     sq_far,
+    ag4_src,
     ag4,
-    low_src,
-    low,
+    fin_src,
+    fin,
     loc,
     tok_s,
     tok_r,
@@ -139,26 +144,22 @@
     rs1_nr,
     rs1_fs,
     rs1_fr,
-    ag2_ns,
-    ag2_nr,
-    ag2_fs,
-    ag2_fr,
+    win_s,
+    win_r,
+    ag2_s,
+    ag2_r,
     att_s,
     att_r,
-    rs3_ns,
-    rs3_nr,
-    rs3_fs,
-    rs3_fr,
-    sq_ns,
-    sq_nr,
-    sq_fs,
-    sq_fr,
-    ag4_ns,
-    ag4_nr,
-    ag4_fs,
-    ag4_fr,
-    low_s,
-    low_r,
+    rs3_s,
+    rs3_r,
+    sq_s,
+    sq_r,
+    mid_s,
+    mid_r,
+    ag4_s,
+    ag4_r,
+    fin_s,
+    fin_r,
     sem_a,
     sem_b,
     sem_c,
@@ -167,8 +168,9 @@
     g, z, t = lax.axis_index("grp"), lax.axis_index("kv"), lax.axis_index("tp")
     ex = Exchange(n_kv, g, z, t)
     count, half = ex.count, ex.half
-    block = tok_all.shape[0] * tok_all.shape[1]
-    mine = tok_all.shape[1]
+    mine = tok_ref.shape[0]
+    block = n_tp * mine
+    all_rows = tok_ref.shape[1]
     head = hgain_ref.shape[1]
     own = n_kv - 1
 
@@ -204,19 +206,23 @@
     first_fetch = len(local)
     fetch(state_hbm, state_v)
     second_fetch = len(local)
-    for h in range(heads):
-        fetch(wo_hbm.at[:, h * head : (h + 1) * head], wo_v.at[h * block : (h + 1) * block])
-    third_fetch = len(local)
-    parts = wu_v.shape[0] // block
-    wide = wu_v.shape[1]
-    for j in range(parts):
-        fetch(wu_hbm.at[:, j * wide : (j + 1) * wide], wu_v.at[j * block : (j + 1) * block])
-    for j in range(parts):
-        fetch(wdn_hbm.at[:, j * wide : (j + 1) * wide], wdn_v.at[j * block : (j + 1) * block])
+    parts = wu_v.shape[1] // (2 * head)
+    wide = 2 * head
+    kinds = heads * seq
+    n_win = len(UP_WINDOW)
+    out_wide = heads * head
+    here_up, here_down = UP_WINDOW.index(0), DOWN_WINDOW.index(0)
+    fetch(wo_hbm, wo_v.at[:, here_up * out_wide : (here_up + 1) * out_wide])
+    fetch(wu_hbm, wu_v.at[here_up * block : (here_up + 1) * block])
+    fetch(wdn_hbm, wdn_v.at[here_down * block : (here_down + 1) * block])
     all_fetch = len(local)
 
     tok_all[t] = tok_ref[...].astype(f32)
+    gain_row = mgain_ref[...].astype(f32).reshape(1, block)
+    gain_row = jnp.concatenate([gain_row, jnp.zeros((1, all_rows - block), f32)], axis=1)
+    tok_all[n_tp] = jnp.broadcast_to(gain_row, (mine, all_rows))
     rhs1[heads * block :, head:] = jnp.zeros((heads * block, head), bf16)
+    diag[...] = jnp.zeros(diag.shape, bf16)
     spread16 = placing(parts * seq, n_kv, seq, z)
     part_of_row = (
         lax.broadcasted_iota(jnp.int32, (n_kv * parts * seq, parts * block), 0) // seq
@@ -224,8 +230,7 @@
     part_mask = part_of_row == (
         lax.broadcasted_iota(jnp.int32, (n_kv * parts * seq, parts * block), 1) // block
     )
-    gain = column_of(gain_ref[...])
-    mixer_gain = column_of(mgain_ref[...])
+    gain = column_of(gain_ref[...].astype(f32).reshape(1, block))
 
     pl.semaphore_wait(barrier, n_tp - 1 + 4)
     for offset in (2, -2):
@@ -278,7 +283,7 @@
         rows = nt(spread16, stacked)
         return jnp.where(part_mask, rows, 0.0).astype(bf16)
 
-    tok_t = tok_all[...].reshape(block, tok_all.shape[2])
+    tok_t = tok_all[0:n_tp].reshape(block, all_rows)
     scaled_t = (tok_t * gain).astype(bf16)
     left = spread(scaled_t)
     both = jnp.concatenate([scaled_t, (tok_t * tok_t).astype(bf16)], axis=0)
@@ -343,9 +348,30 @@
         copies.append((i, reduce_far(i, total, rs1_far_src, rs1_far, rs1_fs, rs1_fr)))
     pending += [c for _, c in copies]
 
+    window = []
+
+    def to_window(src, dst_of, offsets):
+        begun = []
+        for w, offset in enumerate(offsets):
+            if offset:
+                k = len(window)
+                copy = ex.copy(src, dst_of(w), win_s.at[k], win_r.at[k], -offset)
+                copy.start()
+                window.append(copy)
+                begun.append(copy)
+        return begun
+
+    tok_window = to_window(tok_all, lambda w: tok_near.at[w], UP_WINDOW)
+    wo_window = to_window(
+        wo_hbm, lambda w: wo_v.at[:, w * out_wide : (w + 1) * out_wide], UP_WINDOW
+    )
+    wu_window = to_window(wu_hbm, lambda w: wu_v.at[w * block : (w + 1) * block], UP_WINDOW)
+    wdn_window = to_window(
+        wdn_hbm, lambda w: wdn_v.at[w * block : (w + 1) * block], DOWN_WINDOW
+    )
+    pending += window
+
     local[first_fetch].wait()
-    for k in range(second_fetch, third_fetch):
-        local[k].wait()
     sums = far_sum(rs1, rs1_far, copies)
 
     rows = heads * seq
@@ -391,36 +417,17 @@
         * hgain_ref[...]
     )
 
-    def gather_far(buf, send, recv):
-        copies = {}
+    def to_far(src_of, dst, send, recv, sign):
+        copies = []
         for i in ex.farthest_first:
-            copy = ex.copy(
-                buf.at[own], buf.at[2 * count + i], send.at[i], recv.at[i], ex.reach[i]
-            )
+            copy = ex.copy(src_of(i), dst.at[i], send.at[i], recv.at[i], sign * ex.reach[i])
             copy.start()
-            copies[i] = copy
+            copies.append(copy)
         return copies
 
-    def gather_near(buf, copies, send, recv):
-        started = []
-        for i in ex.nearest_first:
-            copies[i].wait_recv()
-            for group, step in ex.near(i):
-                k = group * count + i if group < 2 else 2 * count + i
-                copy = ex.copy(
-                    buf.at[2 * count + i],
-                    buf.at[group * count + i],
-                    send.at[k],
-                    recv.at[k],
-                    step,
-                )
-                copy.start()
-                started.append(copy)
-        return started
-
-    ag2[own] = normed.astype(bf16).astype(f32)
-    copies = gather_far(ag2, ag2_fs, ag2_fr)
-    pending += list(copies.values())
+    ag2_src[...] = normed.astype(bf16)
+    ag2_copies = to_far(lambda i: ag2_src, ag2, ag2_s, ag2_r, 1)
+    pending += ag2_copies
     for k in range(rows):
         matrix = state_v[k % seq, k // seq]
         state_v[k % seq, k // seq] = (
@@ -428,105 +435,173 @@
         )
     store = pltpu.make_async_copy(state_v, state_out, loc.at[all_fetch])
     store.start()
-    spread8 = placing(heads * seq, n_kv, seq, z)
-    head_of_column = (
-        lax.broadcasted_iota(jnp.int32, (block, n_kv * rows), 1) // seq
-    ) % heads
-    started = gather_near(ag2, copies, ag2_ns, ag2_nr)
-    pending += started
-    for copy in started:
-        copy.wait_recv()
-    everyone = ag2[...].reshape(n_kv * rows, head).astype(bf16)
-    by_head = nt(wo_v[...], everyone)
-    chosen = by_head[0:block]
-    for h in range(1, heads):
-        chosen = jnp.where(head_of_column == h, by_head[h * block : (h + 1) * block], chosen)
-    att[t] = exact_nn(chosen, spread8).astype(bf16)
+
+    def iota(shape, dim):
+        return lax.broadcasted_iota(jnp.int32, shape, dim)
+
+    def owner_row(slot, r):
+        half = ex.half
+        reach = jnp.where(slot < half, 2 + 4 * slot, 4 * half - 2 - 4 * slot)
+        return (z - reach + n_kv) % n_kv * seq + r
+
+    per_w = count * seq
+    shape = (n_win * all_rows, all_rows)
+    lane = iota(shape, 1)
+    lane_owner = owner_row(lane % per_w // seq, lane % seq)
+    window_pick = (
+        (lane // per_w == iota(shape, 0) // all_rows) & (lane_owner == iota(shape, 0) % all_rows)
+    ).astype(bf16)
+    shape = (per_w, all_rows)
+    place_rows = (owner_row(iota(shape, 0) // seq, iota(shape, 0) % seq) == iota(shape, 1)).astype(
+        bf16
+    )
+    head_picks = []
+    shape = (per_w, count * kinds)
+    for h in range(heads):
+        r0, c1 = iota(shape, 0), iota(shape, 1)
+        head_picks.append(
+            (
+                (c1 // kinds == r0 // seq) & (c1 % seq == r0 % seq) & (c1 // seq % heads == h)
+            ).astype(bf16)
+        )
+    shape = (count * parts * seq, all_rows)
+    r0, c1 = iota(shape, 0), iota(shape, 1)
+    spread_rows = (
+        (r0 // (parts * seq) == c1 % per_w // seq) & (r0 % seq == c1 % seq)
+    ).astype(bf16)
+    shape = (per_w, count * parts * seq)
+    r0, c1 = iota(shape, 0), iota(shape, 1)
+    part_picks = [
+        (
+            (c1 // (parts * seq) == r0 // seq) & (c1 % seq == r0 % seq) & (c1 // seq % parts == j)
+        ).astype(bf16)
+        for j in range(parts)
+    ]
+    for copy in tok_window:
+        copy.wait_recv()
+    token_parts = []
+    mixer_gain = jnp.zeros((block, all_rows), f32)
+    lane = iota((block, all_rows), 1)
+    for w, offset in enumerate(UP_WINDOW):
+        source = tok_near.at[w] if offset else tok_all
+        token_parts.append(source[0:n_tp].reshape(block, all_rows).astype(bf16))
+        column = column_of(source[n_tp][0:1, 0:block])
+        mixer_gain = jnp.where(lane // per_w == w, column, mixer_gain)
+    token_w = nn(jnp.concatenate(token_parts, axis=1), window_pick)
+    for k in range(second_fetch, all_fetch):
+        local[k].wait()
+    for copy in ag2_copies:
+        copy.wait_recv()
+    for copy in wo_window:
+        copy.wait_recv()
+    everyone = ag2[...].astype(f32).reshape(count * kinds, head).astype(bf16)
+    for h in range(heads):
+        picked = nn(head_picks[h], everyone).astype(bf16)
+        for w in range(n_win):
+            at = w * out_wide + h * head
+            diag[w * per_w : (w + 1) * per_w, at : at + head] = picked
+    att[t] = nt(wo_v[...], diag[...]).astype(bf16)
     copies = to_tp(lambda peer: att.at[t], att, att_s, att_r)
     pending += copies
-    for k in range(third_fetch, all_fetch):
-        local[k].wait()
     for copy in copies:
         copy.wait_recv()
+    for copy in wu_window:
+        copy.wait_recv()
+
     attended = att[0].astype(f32)
     for k in range(1, n_tp):
         attended += att[k].astype(f32)
-    middle = (tok_t + attended).astype(bf16).astype(f32)
-    mid[...] = middle.reshape(mid.shape)
-
-    scaled_t = (middle * mixer_gain).astype(bf16)
-    left = spread(scaled_t)
-    rs3[...] = nn(left, wu_v[...]).astype(bf16).reshape(rs3.shape)
-    started = reduce_near(rs3, rs3_near, rs3_ns, rs3_nr, ex.farthest_first)
-    pending += list(started.values())
-    square_part = jnp.sum(middle * middle, axis=0, keepdims=True)
-    sq_src[...] = square_part
-    sq_started = []
-    for k, step in enumerate((1, -1, 2, -2)):
-        copy = ex.copy(sq_src, sq_near.at[k], sq_ns.at[k], sq_nr.at[k], -step)
-        copy.start()
-        sq_started.append(copy)
-    pending += sq_started
+    middle_b = (token_w + attended).astype(bf16)
+    middle = middle_b.astype(f32)
+    scaled = jnp.concatenate([middle * mixer_gain] * n_win, axis=0)
+    shape = scaled.shape
+    scaled = jnp.where(iota(shape, 1) // per_w == iota(shape, 0) // block, scaled, 0.0)
+    left = nt(spread_rows, scaled.astype(bf16))
+    part = iota(left.shape, 0) // seq % parts
+    product = jnp.zeros((left.shape[0], wide), f32)
+    for j in range(parts):
+        product += nn(
+            jnp.where(part == j, left, 0.0).astype(bf16), wu_v[:, j * wide : (j + 1) * wide]
+        )
+    rs3[...] = product.astype(bf16).reshape(rs3.shape)
+    sq_src[...] = jnp.sum(middle * middle, axis=0, keepdims=True)
+    rs3_copies = to_far(lambda i: rs3.at[i], rs3_far, rs3_s, rs3_r, -1)
+    sq_copies = to_far(lambda i: sq_src, sq_far, sq_s, sq_r, -1)
+    pending += rs3_copies + sq_copies
+    mid_copies = []
+    for w, offset in enumerate(UP_WINDOW):
+        placed = nt(middle_b, window_pick[w * all_rows : (w + 1) * all_rows]).astype(bf16)
+        mid_src[w] = placed.reshape(n_tp, mine, all_rows)
+        if offset:
+            copy = ex.copy(mid_src.at[w, t], mid.at[w], mid_s.at[w], mid_r.at[w], offset)
+            copy.start()
+            mid_copies.append(copy)
+        else:
+            mid[w] = mid_src[w, t]
+    pending += mid_copies
+    for copy in sq_copies:
+        copy.wait_recv()
+    lane = iota((1, all_rows), 1)
+    squares = jnp.zeros((1, all_rows), f32)
+    for i in range(count):
+        squares += jnp.where(lane % per_w // seq == i, sq_far[i], 0.0)
+    shape = (parts * seq, all_rows)
+    squares = jnp.sum(
+        jnp.where(iota(shape, 1) % seq == iota(shape, 0) % seq, squares, 0.0),
+        axis=1,
+        keepdims=True,
+    )
+    second = lax.rsqrt(squares / width + epsilon)
+    up = jnp.zeros((parts * seq, wide), f32)
+    for copy in reversed(rs3_copies):
+        copy.wait_recv()
+    for i in range(count):
+        up += rs3_far[i].astype(f32)
+    ag4_src[...] = jnp.square(jnp.maximum(second * up, 0.0)).astype(bf16)
+
+    ag4_copies = to_far(lambda i: ag4_src, ag4, ag4_s, ag4_r, 1)
+    pending += ag4_copies
+    for copy in wdn_window:
+        copy.wait_recv()
+    for copy in mid_copies:
+        copy.wait_recv()
+    middle = mid[0].astype(f32)
+    for w in range(1, n_win):
+        middle += mid[w].astype(f32)
+    for copy in ag4_copies:
+        copy.wait_recv()
+    everyone = ag4[...].reshape(count * parts * seq, wide)
+    picked = jnp.concatenate(
+        [nn(part_picks[j], everyone).astype(bf16) for j in range(parts)], axis=1
+    )
+    lowered_part = nt(wdn_v[...], picked).astype(bf16)
+    fin_src[...] = nn(lowered_part, place_rows).astype(bf16).reshape(fin_src.shape)
     copies = []
-    for i in ex.farthest_first:
-        total = near_sum(i, rs3, rs3_near, started)
-        copies.append((i, reduce_far(i, total, rs3_far_src, rs3_far, rs3_fs, rs3_fr)))
-    pending += [c for _, c in copies]
-    for copy in sq_started:
-        copy.wait_recv()
-    base = square_part + sq_near[0] + sq_near[1]
-    sq_far_src[0] = base + sq_near[2]
-    sq_far_src[1] = base + sq_near[3]
-    sq_far_src[2] = base
-    sq_copies = []
-    for i in ex.farthest_first:
-        which_sum = 2 if i == count - 1 else (0 if i < half else 1)
-        copy = ex.copy(
-            sq_far_src.at[which_sum], sq_far.at[i], sq_fs.at[i], sq_fr.at[i], -ex.reach[i]
-        )
-        copy.start()
-        sq_copies.append(copy)
-    pending += sq_copies
-    for copy in sq_copies:
-        copy.wait_recv()
-    square_two = square_part
-    for i in range(count):
-        square_two += sq_far[i]
-    second_all = lax.rsqrt(square_two / width + epsilon)
-    row_of = z * seq + lax.broadcasted_iota(
-        jnp.int32, (parts * seq, second_all.shape[1]), 0
-    ) % seq
-    lane_of = lax.broadcasted_iota(jnp.int32, (parts * seq, second_all.shape[1]), 1)
-    second = jnp.sum(jnp.where(lane_of == row_of, second_all, 0.0), axis=1, keepdims=True)
-    up = far_sum(rs3, rs3_far, copies)
-    hidden = jnp.square(jnp.maximum(second * up, 0.0)).astype(bf16)
-
-    ag4[own] = hidden
-    copies = gather_far(ag4, ag4_fs, ag4_fr)
-    pending += list(copies.values())
-    started = gather_near(ag4, copies, ag4_ns, ag4_nr)
-    pending += started
-    for copy in started:
-        copy.wait_recv()
-    everyone = ag4[...].reshape(n_kv * parts * seq, wide)
-    by_part = nt(wdn_v[...], everyone)
-    part_of_column = (
-        lax.broadcasted_iota(jnp.int32, (block, n_kv * parts * seq), 1) // seq
-    ) % parts
-    chosen = by_part[0:block]
-    for j in range(1, parts):
-        chosen = jnp.where(part_of_column == j, by_part[j * block : (j + 1) * block], chosen)
-    lowered_part = exact_nn(chosen, spread16).astype(bf16).astype(f32)
-    low_src[...] = lowered_part.reshape(low_src.shape)
-    copies = to_tp(lambda peer: low_src.at[peer], low, low_s, low_r)
+    for w, offset in enumerate(DOWN_WINDOW):
+        row = lax.rem(z + offset + n_kv, n_kv)
+        for k in range(n_tp):
+            if offset == 0 and k == 0:
+                fin[w, t] = fin_src[w, t]
+                continue
+            peer = lax.rem(t + k, n_tp)
+            copy = pltpu.make_async_remote_copy(
+                src_ref=fin_src.at[w, peer],
+                dst_ref=fin.at[w, t],
+                send_sem=fin_s.at[w * n_tp + k],
+                recv_sem=fin_r.at[w * n_tp + k],
+                device_id=(g, row, peer),
+                device_id_type=MESH,
+            )
+            copy.start()
+            copies.append(copy)
     pending += copies
-    low[t] = low_src[t]
     for copy in copies:
         copy.wait_recv()
-    lowered = low[0]
-    for k in range(1, n_tp):
-        lowered += low[k]
-    out_ref[...] = (mid[t] + lowered).astype(bf16)
+    lowered = jnp.zeros((mine, all_rows), f32)
+    for w in range(n_win):
+        for k in range(n_tp):
+            lowered += fin[w, k].astype(f32)
+    out_ref[...] = (middle + lowered).astype(bf16)
     for copy in pending:
         copy.wait_send()
     store.wait()
@@ -555,7 +630,7 @@
         seq, heads, head = state.shape[:3]
         rows, mine = tokens.shape
         block = w_query.shape[0]
-        parts = w_up.shape[1] * seq * n_kv // (rows * 2 * head)
+        parts = w_up.shape[1] // (2 * head)
         wide = w_up.shape[1] // parts
         count = n_kv // 4
         dims = (n_kv, n_tp, seq, heads, block * n_kv)
@@ -567,60 +642,59 @@
         dma = pltpu.SemaphoreType.DMA
         blocks = (parts * seq, wide)
         near = (3 * count - 1,)
-        n_local = 3 * heads + 2 + 1 + heads + 2 * parts + 1
+        far = (count,)
+        n_local = 3 * heads + 2 + 1 + 3 + 1
+        n_win = len(UP_WINDOW)
         scratch = [
-            pltpu.VMEM((n_tp, mine, rows), f32),
+            pltpu.VMEM((n_tp + 1, mine, rows), f32),
+            pltpu.VMEM((n_win, n_tp + 1, mine, rows), f32),
             pltpu.VMEM(state.shape, f32),
             pltpu.VMEM((2 * heads * block, 2 * head), bf16),
             pltpu.VMEM((2, w_beta.shape[1], head), bf16),
-            pltpu.VMEM((heads * block, head), bf16),
-            pltpu.VMEM((parts * block, wide), bf16),
-            pltpu.VMEM((parts * block, wide), bf16),
+            pltpu.VMEM((block, n_win * heads * head), bf16),
+            pltpu.VMEM((n_win * block, w_up.shape[1]), bf16),
+            pltpu.VMEM((n_win * block, w_down.shape[0]), bf16),
             pltpu.VMEM((n_kv, *blocks), bf16),
-            pltpu.VMEM((3 * count - 1, *blocks), bf16),
+            pltpu.VMEM((*near, *blocks), bf16),
             pltpu.VMEM((count, *blocks), bf16),
             pltpu.VMEM((count, *blocks), bf16),
-            pltpu.VMEM((n_kv, heads * seq, head), f32),
+            pltpu.VMEM((heads * seq, head), bf16),
+            pltpu.VMEM((count, heads * seq, head), bf16),
+            pltpu.VMEM((rows, n_win * heads * head), bf16),
             pltpu.VMEM((n_tp, block, rows), bf16),
-            pltpu.VMEM((n_tp, mine, rows), f32),
-            pltpu.VMEM((n_kv, *blocks), bf16),
-            pltpu.VMEM((3 * count - 1, *blocks), bf16),
+            pltpu.VMEM((n_win, n_tp, mine, rows), bf16),
+            pltpu.VMEM((n_win, mine, rows), bf16),
             pltpu.VMEM((count, *blocks), bf16),
             pltpu.VMEM((count, *blocks), bf16),
             pltpu.VMEM((1, rows), f32),
-            pltpu.VMEM((4, 1, rows), f32),
-            pltpu.VMEM((3, 1, rows), f32),
             pltpu.VMEM((count, 1, rows), f32),
-            pltpu.VMEM((n_kv, *blocks), bf16),
-            pltpu.VMEM((n_tp, mine, rows), f32),
-            pltpu.VMEM((n_tp, mine, rows), f32),
+            pltpu.VMEM(blocks, bf16),
+            pltpu.VMEM((count, *blocks), bf16),
+            pltpu.VMEM((n_win, n_tp, mine, rows), bf16),
+            pltpu.VMEM((n_win, n_tp, mine, rows), bf16),
             dma((n_local,)),
             dma((n_tp - 1,)),
             dma((n_tp - 1,)),
             dma(near),
             dma(near),
-            dma((count,)),
-            dma((count,)),
-            dma(near),
-            dma(near),
-            dma((count,)),
-            dma((count,)),
+            dma(far),
+            dma(far),
+            dma((4 * (n_win - 1),)),
+            dma((4 * (n_win - 1),)),
+            dma(far),
+            dma(far),
             dma((n_tp - 1,)),
             dma((n_tp - 1,)),
-            dma(near),
-            dma(near),
-            dma((count,)),
-            dma((count,)),
-            dma((4,)),
-            dma((4,)),
-            dma((count,)),
-            dma((count,)),
-            dma(near),
-            dma(near),
-            dma((count,)),
-            dma((count,)),
-            dma((n_tp - 1,)),
-            dma((n_tp - 1,)),
+            dma(far),
+            dma(far),
+            dma(far),
+            dma(far),
+            dma((n_win,)),
+            dma((n_win,)),
+            dma(far),
+            dma(far),
+            dma((n_win * n_tp,)),
+            dma((n_win * n_tp,)),
             pltpu.SemaphoreType.REGULAR,
             pltpu.SemaphoreType.REGULAR,
             pltpu.SemaphoreType.REGULAR,
@@ -654,7 +728,7 @@
         )(
             tokens.T,
             state,
-            norm_gain.astype(f32).reshape(1, block),
+            norm_gain,
             w_query,
             w_key,
             w_value,
@@ -664,7 +738,7 @@
             dt_bias,
             head_gain.reshape(1, head),
             w_out.T,
-            mixer_gain.astype(f32).reshape(1, block),
+            mixer_gain,
             w_up,
             w_down.T,
         )

time: 135 us -> 130 us (0.963)
  Pallas kernels: 130 us -> 126 us
    pallas_call x1, Pallas kernels: 130 us -> 126 us  [local(): pl.pallas_call(functools.partial(kernel, dims), out_shape=(jax.ShapeDtype...]
    unnamed x8 -> x4, local copies, waits for them, and re-layouts: 3.77 us -> 3.11 us
where the time goes in v3:
time: 130 us; the launch traced here: 129 us
  Pallas kernels  126 us (97%)
  local copies, waits for them, and re-layouts  3.11 us (2%)
    pallas_call x1, Pallas kernels, local(): pl.pallas_call(functools.partial(kernel, dims), out_shape=(jax.ShapeDtype...  126 us
    unnamed x4, local copies, waits for them, and re-layouts  3.11 us

profile of v3, /device:TPU:33, one launch (start us, length us, event | category | flops | bytes accessed | tf_op | source)
XLA Modules:
  0.0 129.4 jit_solution(12973648375404510152)
XLA Ops:
  0.6 125.7 %shard_map.158 = (bf16[8,128]{1,0:T(8,128)(2,1)}, f32[4,2,128,128]{3,2,1,0:T(8,128)}) custom-call(bf16[8,128]{1,0:T(8,128)(2,1)} %bitcast.11, f32[4,2,128,128]{3,2,1,0:T(8,128)} %state_hbm.1, bf16[64]{0:T(256)(128)(2,1)} %gain_ref.1, bf16[64,256]{1,0:T(8,128)(2,1)} %wq_hbm.1, bf16[64,256]{1,0:T(8,128)(2,1)} %wk_hbm.1, bf16[64,256]{1,0:T(8,128)(2,1)} %wv_hbm.1, ...), custom_call_target="tpu_custom_call" | custom-call | tf_op jit(solution)/shard_map/pallas_call | solution.py:702
  126.3 0.0 copy-start
  126.3 0.7 copy-done
  127.0 0.6 copy.19
  127.6 1.9 %copy.20 = f32[4,2,128,128]{3,2,1,0:T(8,128)} copy(f32[4,2,128,128]{3,2,1,0:T(8,128)} %get-tuple-element.9) | data formatting | bytes 1048576
Async XLA Ops:
  126.3 0.7 copy-start

commit v4 on v3

--- a/solution.py
+++ b/solution.py
@@ -217,10 +217,10 @@
     fetch(wdn_hbm, wdn_v.at[here_down * block : (here_down + 1) * block])
     all_fetch = len(local)
 
-    tok_all[t] = tok_ref[...].astype(f32)
+    tok_all[t] = tok_ref[...]
     gain_row = mgain_ref[...].astype(f32).reshape(1, block)
     gain_row = jnp.concatenate([gain_row, jnp.zeros((1, all_rows - block), f32)], axis=1)
-    tok_all[n_tp] = jnp.broadcast_to(gain_row, (mine, all_rows))
+    tok_all[n_tp] = jnp.broadcast_to(gain_row, (mine, all_rows)).astype(bf16)
     rhs1[heads * block :, head:] = jnp.zeros((heads * block, head), bf16)
     diag[...] = jnp.zeros(diag.shape, bf16)
     spread16 = placing(parts * seq, n_kv, seq, z)
@@ -283,7 +283,7 @@
         rows = nt(spread16, stacked)
         return jnp.where(part_mask, rows, 0.0).astype(bf16)
 
-    tok_t = tok_all[0:n_tp].reshape(block, all_rows)
+    tok_t = tok_all[0:n_tp].astype(f32).reshape(block, all_rows)
     scaled_t = (tok_t * gain).astype(bf16)
     left = spread(scaled_t)
     both = jnp.concatenate([scaled_t, (tok_t * tok_t).astype(bf16)], axis=0)
@@ -365,11 +365,6 @@
     wo_window = to_window(
         wo_hbm, lambda w: wo_v.at[:, w * out_wide : (w + 1) * out_wide], UP_WINDOW
     )
-    wu_window = to_window(wu_hbm, lambda w: wu_v.at[w * block : (w + 1) * block], UP_WINDOW)
-    wdn_window = to_window(
-        wdn_hbm, lambda w: wdn_v.at[w * block : (w + 1) * block], DOWN_WINDOW
-    )
-    pending += window
 
     local[first_fetch].wait()
     sums = far_sum(rs1, rs1_far, copies)
@@ -428,13 +423,16 @@
     ag2_src[...] = normed.astype(bf16)
     ag2_copies = to_far(lambda i: ag2_src, ag2, ag2_s, ag2_r, 1)
     pending += ag2_copies
+    wu_window = to_window(wu_hbm, lambda w: wu_v.at[w * block : (w + 1) * block], UP_WINDOW)
+    wdn_window = to_window(
+        wdn_hbm, lambda w: wdn_v.at[w * block : (w + 1) * block], DOWN_WINDOW
+    )
+    pending += window
     for k in range(rows):
         matrix = state_v[k % seq, k // seq]
-        state_v[k % seq, k // seq] = (
+        state_out[k % seq, k // seq] = (
             decay[k : k + 1] * matrix + key_t[:, k : k + 1] * fresh[k : k + 1]
         )
-    store = pltpu.make_async_copy(state_v, state_out, loc.at[all_fetch])
-    store.start()
 
     def iota(shape, dim):
         return lax.broadcasted_iota(jnp.int32, shape, dim)
@@ -484,8 +482,8 @@
     lane = iota((block, all_rows), 1)
     for w, offset in enumerate(UP_WINDOW):
         source = tok_near.at[w] if offset else tok_all
-        token_parts.append(source[0:n_tp].reshape(block, all_rows).astype(bf16))
-        column = column_of(source[n_tp][0:1, 0:block])
+        token_parts.append(source[0:n_tp].astype(f32).reshape(block, all_rows).astype(bf16))
+        column = column_of(source[n_tp].astype(f32)[0:1, 0:block])
         mixer_gain = jnp.where(lane // per_w == w, column, mixer_gain)
     token_w = nn(jnp.concatenate(token_parts, axis=1), window_pick)
     for k in range(second_fetch, all_fetch):
@@ -604,7 +602,6 @@
     out_ref[...] = (middle + lowered).astype(bf16)
     for copy in pending:
         copy.wait_send()
-    store.wait()
 
 
 def solution(mesh):
@@ -636,7 +633,7 @@
         dims = (n_kv, n_tp, seq, heads, block * n_kv)
         vmem, hbm, smem = (
             pl.BlockSpec(memory_space=pltpu.VMEM),
-            pl.BlockSpec(memory_space=pl.ANY),
+            pl.BlockSpec(memory_space=pltpu.HBM),
             pl.BlockSpec(memory_space=pltpu.SMEM),
         )
         dma = pltpu.SemaphoreType.DMA
@@ -646,8 +643,8 @@
         n_local = 3 * heads + 2 + 1 + 3 + 1
         n_win = len(UP_WINDOW)
         scratch = [
-            pltpu.VMEM((n_tp + 1, mine, rows), f32),
-            pltpu.VMEM((n_win, n_tp + 1, mine, rows), f32),
+            pltpu.VMEM((n_tp + 1, mine, rows), bf16),
+            pltpu.VMEM((n_win, n_tp + 1, mine, rows), bf16),
             pltpu.VMEM(state.shape, f32),
             pltpu.VMEM((2 * heads * block, 2 * head), bf16),
             pltpu.VMEM((2, w_beta.shape[1], head), bf16),
@@ -722,25 +719,25 @@
                 hbm,
                 hbm,
             ],
-            out_specs=(vmem, hbm),
+            out_specs=(vmem, vmem),
             scratch_shapes=scratch,
-            compiler_params=pltpu.CompilerParams(collective_id=0, has_side_effects=True),
+            compiler_params=pltpu.CompilerParams(collective_id=0, has_side_effects=True, vmem_limit_bytes=32 * 2**20),
         )(
             tokens.T,
-            state,
+            pltpu.with_memory_space_constraint(state, pltpu.HBM),
             norm_gain,
-            w_query,
-            w_key,
-            w_value,
-            w_beta.T,
-            w_decay.T,
+            pltpu.with_memory_space_constraint(w_query, pltpu.HBM),
+            pltpu.with_memory_space_constraint(w_key, pltpu.HBM),
+            pltpu.with_memory_space_constraint(w_value, pltpu.HBM),
+            pltpu.with_memory_space_constraint(w_beta.T, pltpu.HBM),
+            pltpu.with_memory_space_constraint(w_decay.T, pltpu.HBM),
             a_log,
             dt_bias,
             head_gain.reshape(1, head),
-            w_out.T,
+            pltpu.with_memory_space_constraint(w_out.T, pltpu.HBM),
             mixer_gain,
-            w_up,
-            w_down.T,
+            pltpu.with_memory_space_constraint(w_up, pltpu.HBM),
+            pltpu.with_memory_space_constraint(w_down.T, pltpu.HBM),
         )
         return mixed_t.T, new_state
 

time: 130 us -> 123 us (0.946)
  Pallas kernels: 126 us -> 120 us
    pallas_call x1, Pallas kernels: 126 us -> 120 us  [local(): pl.pallas_call(functools.partial(kernel, dims), out_shape=(jax.ShapeDtype...]
    unnamed x4 -> x14, local copies, waits for them, and re-layouts: 3.11 us -> 2.06 us
where the time goes in v4:
time: 123 us
  Pallas kernels  120 us (98%)
  local copies, waits for them, and re-layouts  2.06 us (2%)
    pallas_call x1, Pallas kernels, local(): pl.pallas_call(functools.partial(kernel, dims), out_shape=(jax.ShapeDtype...  120 us

profile of v4, /device:TPU:33, one launch (start us, length us, event | category | flops | bytes accessed | tf_op | source)
XLA Modules:
  0.0 122.9 jit_solution(2040029816820580252)
XLA Ops:
  0.6 0.0 copy-start.4
  0.6 0.0 copy-start.5
  0.7 0.0 copy-start
  0.7 0.0 copy-start.1
  0.7 0.0 copy-start.2
  0.7 0.0 copy-start.3
  0.7 0.6 copy-done.4
  1.3 0.0 copy-done.5
  1.3 0.0 copy-done
  1.4 0.0 copy-done.1
  1.4 0.0 copy-done.2
  1.4 0.0 copy-done.3
  1.4 120.1 %shard_map.158 = (bf16[8,128]{1,0:T(8,128)(2,1)S(1)}, f32[4,2,128,128]{3,2,1,0:T(8,128)S(1)}) custom-call(bf16[8,128]{1,0:T(8,128)(2,1)S(1)} %bitcast.7, f32[4,2,128,128]{3,2,1,0:T(8,128)} %state_hbm.1, bf16[64]{0:T(256)(128)(2,1)S(1)} %copy-done.1, bf16[64,256]{1,0:T(8,128)(2,1)} %wq_hbm.1, bf16[64,256]{1,0:T(8,128)(2,1)} %wk_hbm.1, ...), custom_call_target="tpu_custom_call" | custom-call | tf_op jit(solution)/shard_map/pallas_call | solution.py:699
  121.5 0.6 copy.19
  122.1 0.8 copy.20
Async XLA Ops:
  0.6 0.7 copy-start.4
  0.6 0.7 copy-start.5
  0.7 0.7 copy-start
  0.7 0.7 copy-start.1
  0.7 0.7 copy-start.2
  0.7 0.7 copy-start.3

commit v5 on v4

--- a/solution.py
+++ b/solution.py
@@ -137,6 +137,11 @@
     ag4,
     fin_src,
     fin,
+    gain_v,
+    mgain_v,
+    hgain_v,
+    alog_v,
+    dt_v,
     loc,
     tok_s,
     tok_r,
@@ -171,7 +176,7 @@
     mine = tok_ref.shape[0]
     block = n_tp * mine
     all_rows = tok_ref.shape[1]
-    head = hgain_ref.shape[1]
+    head = hgain_v.shape[1]
     own = n_kv - 1
 
     def tp_peer(k):
@@ -183,44 +188,60 @@
     for offset in (1, -1, 2, -2):
         pl.semaphore_signal(barrier, inc=1, device_id=ex.device(offset), device_id_type=MESH)
 
-    local = []
-
-    def fetch(src, dst):
-        copy = pltpu.make_async_copy(src, dst, loc.at[len(local)])
+    def waiter(ref, send, recv):
+        return pltpu.make_async_remote_copy(
+            src_ref=ref,
+            dst_ref=ref,
+            send_sem=send,
+            recv_sem=recv,
+            device_id=tp_peer(1),
+            device_id_type=MESH,
+        )
+
+    def fetch(src, dst, k):
+        copy = pltpu.make_async_copy(src, dst, loc.at[k])
         copy.start()
-        local.append(copy)
-
+        return copy
+
+    got_tok = fetch(tok_ref, tok_all.at[t], 0)
+    got_mgain = fetch(mgain_ref, mgain_v, 1)
+    got_gain = fetch(gain_ref, gain_v, 2)
+    lanes = wext.shape[2]
+    at = pl.multiple_of((z * block // lanes) * lanes, lanes)
+    got_ext = [
+        fetch(wb_hbm.at[:, pl.ds(at, lanes)], wext.at[0], 3),
+        fetch(wd_hbm.at[:, pl.ds(at, lanes)], wext.at[1], 4),
+    ]
     for i, w in enumerate((wq_hbm, wk_hbm)):
         for h in range(heads):
             at = (i * heads + h) * block
-            fetch(w.at[:, h * head : (h + 1) * head], rhs1.at[at : at + block, 0:head])
+            fetch(w.at[:, h * head : (h + 1) * head], rhs1.at[at : at + block, 0:head], 5)
     for h in range(heads):
         fetch(
             wv_hbm.at[:, h * head : (h + 1) * head],
             rhs1.at[h * block : (h + 1) * block, head : 2 * head],
+            5,
         )
-    lanes = wext.shape[2]
-    at = pl.multiple_of((z * block // lanes) * lanes, lanes)
-    fetch(wb_hbm.at[:, pl.ds(at, lanes)], wext.at[0])
-    fetch(wd_hbm.at[:, pl.ds(at, lanes)], wext.at[1])
-    first_fetch = len(local)
-    fetch(state_hbm, state_v)
-    second_fetch = len(local)
+    whole = rhs1.at[0 : 3 * heads * block // 2]
+    got_rhs1 = pltpu.make_async_copy(whole, whole, loc.at[5])
+    got_small = [
+        fetch(hgain_ref, hgain_v, 6),
+        fetch(alog_ref, alog_v, 7),
+        fetch(dt_ref, dt_v, 8),
+    ]
+    got_state = fetch(state_hbm, state_v, 9)
     parts = wu_v.shape[1] // (2 * head)
     wide = 2 * head
     kinds = heads * seq
     n_win = len(UP_WINDOW)
     out_wide = heads * head
     here_up, here_down = UP_WINDOW.index(0), DOWN_WINDOW.index(0)
-    fetch(wo_hbm, wo_v.at[:, here_up * out_wide : (here_up + 1) * out_wide])
-    fetch(wu_hbm, wu_v.at[here_up * block : (here_up + 1) * block])
-    fetch(wdn_hbm, wdn_v.at[here_down * block : (here_down + 1) * block])
-    all_fetch = len(local)
-
-    tok_all[t] = tok_ref[...]
-    gain_row = mgain_ref[...].astype(f32).reshape(1, block)
-    gain_row = jnp.concatenate([gain_row, jnp.zeros((1, all_rows - block), f32)], axis=1)
-    tok_all[n_tp] = jnp.broadcast_to(gain_row, (mine, all_rows)).astype(bf16)
+    got_weights = [
+        fetch(wo_hbm, wo_v.at[:, here_up * out_wide : (here_up + 1) * out_wide], 10),
+        fetch(wu_hbm, wu_v.at[here_up * block : (here_up + 1) * block], 11),
+        fetch(wdn_hbm, wdn_v.at[here_down * block : (here_down + 1) * block], 12),
+    ]
+
     rhs1[heads * block :, head:] = jnp.zeros((heads * block, head), bf16)
     diag[...] = jnp.zeros(diag.shape, bf16)
     spread16 = placing(parts * seq, n_kv, seq, z)
@@ -230,33 +251,37 @@
     part_mask = part_of_row == (
         lax.broadcasted_iota(jnp.int32, (n_kv * parts * seq, parts * block), 1) // block
     )
-    gain = column_of(gain_ref[...].astype(f32).reshape(1, block))
+    got_mgain.wait()
+    gain_row = mgain_v[...].astype(f32).reshape(1, block)
+    gain_row = jnp.concatenate([gain_row, jnp.zeros((1, all_rows - block), f32)], axis=1)
+    tok_all[n_tp] = jnp.broadcast_to(gain_row, (mine, all_rows)).astype(bf16)
+    got_gain.wait()
+    gain = column_of(gain_v[...].astype(f32).reshape(1, block))
+    got_tok.wait()
 
     pl.semaphore_wait(barrier, n_tp - 1 + 4)
     for offset in (2, -2):
         pl.semaphore_signal(sem_a, inc=1, device_id=ex.device(offset), device_id_type=MESH)
 
-    def to_tp(src_of, dst, send, recv):
-        copies = []
+    def to_tp(dst, send, recv):
         for k in range(1, n_tp):
             peer = lax.rem(t + k, n_tp)
-            copy = pltpu.make_async_remote_copy(
-                src_ref=src_of(peer),
+            pltpu.make_async_remote_copy(
+                src_ref=dst.at[t],
                 dst_ref=dst.at[t],
-                send_sem=send.at[k - 1],
-                recv_sem=recv.at[k - 1],
+                send_sem=send,
+                recv_sem=recv,
                 device_id=(g, z, peer),
                 device_id_type=MESH,
-            )
-            copy.start()
-            copies.append(copy)
-        return copies
+            ).start()
+        return waiter(dst.at[0 : n_tp - 1], send, recv)
 
     pending = []
-    copies = to_tp(lambda peer: tok_all.at[t], tok_all, tok_s, tok_r)
-    pending += copies
-    for k in range(first_fetch):
-        local[k].wait()
+    tok_sent = to_tp(tok_all, tok_s, tok_r)
+    pending.append(tok_sent)
+    got_rhs1.wait()
+    for copy in got_ext:
+        copy.wait()
     odd = lax.rem(z, lanes // block) if lanes // block > 1 else 0
     pieces = []
     for i in range(2):
@@ -275,8 +300,7 @@
     pl.semaphore_wait(sem_a, 2)
     for offset in (4, -4):
         pl.semaphore_signal(sem_b, inc=1, device_id=ex.device(offset), device_id_type=MESH)
-    for copy in copies:
-        copy.wait_recv()
+    tok_sent.wait_recv()
 
     def spread(x_t):
         stacked = jnp.concatenate([x_t] * parts, axis=0)
@@ -294,80 +318,61 @@
     product = jnp.concatenate([product[:, :head], product[:, head:] + extra], axis=1)
     rs1[...] = product.astype(bf16).reshape(rs1.shape)
 
-    def reduce_near(buf, near_buf, send, recv, order):
-        started = {}
-        for i in order:
-            for group, step in ex.near(i):
-                k = group * count + i if group < 2 else 2 * count + i
-                copy = ex.copy(
-                    buf.at[group * count + i],
-                    near_buf.at[k],
-                    send.at[k],
-                    recv.at[k],
-                    -step,
-                )
-                copy.start()
-                started[k] = copy
-        return started
-
-    def near_sum(i, buf, near_buf, started):
-        total = buf[2 * count + i].astype(f32)
+    for i in ex.farthest_first:
         for group, step in ex.near(i):
             k = group * count + i if group < 2 else 2 * count + i
-            started[k].wait_recv()
-            total += near_buf[k].astype(f32)
-        return total
-
-    def reduce_far(i, total, far_src, far_buf, send, recv):
-        far_src[i] = total.astype(far_src.dtype)
-        copy = ex.copy(far_src.at[i], far_buf.at[i], send.at[i], recv.at[i], -ex.reach[i])
-        copy.start()
-        return copy
-
-    def far_sum(buf, far_buf, copies):
-        total = buf[own].astype(f32)
-        for i, copy in copies:
-            copy.wait_recv()
-            total += far_buf[i].astype(f32)
-        return total
-
-    close = [i for i in ex.nearest_first if abs(ex.reach[i]) <= 8]
-    distant = [i for i in ex.farthest_first if abs(ex.reach[i]) > 8]
-    started = reduce_near(rs1, rs1_near, rs1_ns, rs1_nr, distant + close)
-    pending += list(started.values())
+            ex.copy(
+                rs1.at[group * count + i], rs1_near.at[k], rs1_ns, rs1_nr, -step
+            ).start()
+    near_sent = waiter(rs1.at[0 : 3 * count - 1], rs1_ns, rs1_nr)
+    pending.append(near_sent)
     pl.semaphore_wait(sem_b, 2)
     for offset in (8, -8):
         pl.semaphore_signal(sem_c, inc=1, device_id=ex.device(offset), device_id_type=MESH)
-    copies = []
-    for i in close:
-        total = near_sum(i, rs1, rs1_near, started)
-        copies.append((i, reduce_far(i, total, rs1_far_src, rs1_far, rs1_fs, rs1_fr)))
-    totals = [near_sum(i, rs1, rs1_near, started) for i in distant]
+    near_sent.wait_recv()
+    for i in range(count):
+        total = rs1[2 * count + i].astype(f32)
+        for group, step in ex.near(i):
+            k = group * count + i if group < 2 else 2 * count + i
+            total += rs1_near[k].astype(f32)
+        rs1_far_src[i] = total.astype(bf16)
     pl.semaphore_wait(sem_c, 2)
-    for i, total in zip(distant, totals):
-        copies.append((i, reduce_far(i, total, rs1_far_src, rs1_far, rs1_fs, rs1_fr)))
-    pending += [c for _, c in copies]
-
-    window = []
-
-    def to_window(src, dst_of, offsets):
-        begun = []
+
+    def to_far(src_of, dst, send, recv, sign):
+        for i in ex.farthest_first:
+            ex.copy(src_of(i), dst.at[i], send, recv, sign * ex.reach[i]).start()
+        sent = waiter(dst, send, recv)
+        pending.append(sent)
+        return sent
+
+    far_sent = to_far(lambda i: rs1_far_src.at[i], rs1_far, rs1_fs, rs1_fr, -1)
+
+    def to_window(src, dst_of, whole, k, offsets):
         for w, offset in enumerate(offsets):
             if offset:
-                k = len(window)
-                copy = ex.copy(src, dst_of(w), win_s.at[k], win_r.at[k], -offset)
-                copy.start()
-                window.append(copy)
-                begun.append(copy)
-        return begun
-
-    tok_window = to_window(tok_all, lambda w: tok_near.at[w], UP_WINDOW)
+                ex.copy(src, dst_of(w), win_s.at[k], win_r.at[k], -offset).start()
+        sent = waiter(whole, win_s.at[k], win_r.at[k])
+        pending.append(sent)
+        return sent
+
+    tok_window = to_window(
+        tok_all, lambda w: tok_near.at[w], tok_near.at[0 : n_win - 1], 0, UP_WINDOW
+    )
     wo_window = to_window(
-        wo_hbm, lambda w: wo_v.at[:, w * out_wide : (w + 1) * out_wide], UP_WINDOW
-    )
-
-    local[first_fetch].wait()
-    sums = far_sum(rs1, rs1_far, copies)
+        wo_hbm,
+        lambda w: wo_v.at[:, w * out_wide : (w + 1) * out_wide],
+        wo_v.at[:, 0 : (n_win - 1) * out_wide],
+        1,
+        UP_WINDOW,
+    )
+
+    got_state.wait()
+    for copy in got_small:
+        copy.wait()
+    far_sent.wait_recv()
+    sums = rs1[own].astype(f32)
+    for i in range(count):
+        sums += rs1_far[i].astype(f32)
 
     rows = heads * seq
     query_sum, key_sum = sums[:rows, :head], sums[rows:, :head]
@@ -387,11 +392,12 @@
     key = key_pre * lax.rsqrt(jnp.sum(key_pre * key_pre, axis=1, keepdims=True) + epsilon)
     beta = jax.nn.sigmoid(first * beta_sum)
     which1 = lax.broadcasted_iota(jnp.int32, (rows, 1), 0) // seq
+    a_logs, dt_biases = alog_v[...].reshape(1, heads), dt_v[...].reshape(1, heads)
     a_log = jnp.zeros((rows, 1), f32)
     dt_bias = jnp.zeros((rows, 1), f32)
     for h in range(heads):
-        a_log = jnp.where(which1 == h, alog_ref[h], a_log)
-        dt_bias = jnp.where(which1 == h, dt_ref[h], dt_bias)
+        a_log = jnp.where(which1 == h, a_logs[:, h : h + 1], a_log)
+        dt_bias = jnp.where(which1 == h, dt_biases[:, h : h + 1], dt_bias)
     logit = first * decay_sum + dt_bias
     softplus = jnp.maximum(logit, 0.0) + jnp.log1p(jnp.exp(-jnp.abs(logit)))
     decay = jnp.exp(-jnp.exp(a_log) * softplus)
@@ -409,25 +415,25 @@
     normed = (
         reading
         * lax.rsqrt(jnp.mean(reading * reading, axis=1, keepdims=True) + epsilon)
-        * hgain_ref[...]
-    )
-
-    def to_far(src_of, dst, send, recv, sign):
-        copies = []
-        for i in ex.farthest_first:
-            copy = ex.copy(src_of(i), dst.at[i], send.at[i], recv.at[i], sign * ex.reach[i])
-            copy.start()
-            copies.append(copy)
-        return copies
+        * hgain_v[...]
+    )
 
     ag2_src[...] = normed.astype(bf16)
-    ag2_copies = to_far(lambda i: ag2_src, ag2, ag2_s, ag2_r, 1)
-    pending += ag2_copies
-    wu_window = to_window(wu_hbm, lambda w: wu_v.at[w * block : (w + 1) * block], UP_WINDOW)
+    ag2_sent = to_far(lambda i: ag2_src, ag2, ag2_s, ag2_r, 1)
+    wu_window = to_window(
+        wu_hbm,
+        lambda w: wu_v.at[w * block : (w + 1) * block],
+        wu_v.at[0 : (n_win - 1) * block],
+        2,
+        UP_WINDOW,
+    )
     wdn_window = to_window(
-        wdn_hbm, lambda w: wdn_v.at[w * block : (w + 1) * block], DOWN_WINDOW
-    )
-    pending += window
+        wdn_hbm,
+        lambda w: wdn_v.at[w * block : (w + 1) * block],
+        wdn_v.at[0 : (n_win - 1) * block],
+        3,
+        DOWN_WINDOW,
+    )
     for k in range(rows):
         matrix = state_v[k % seq, k // seq]
         state_out[k % seq, k // seq] = (
@@ -475,8 +481,7 @@
         ).astype(bf16)
         for j in range(parts)
     ]
-    for copy in tok_window:
-        copy.wait_recv()
+    tok_window.wait_recv()
     token_parts = []
     mixer_gain = jnp.zeros((block, all_rows), f32)
     lane = iota((block, all_rows), 1)
@@ -486,12 +491,10 @@
         column = column_of(source[n_tp].astype(f32)[0:1, 0:block])
         mixer_gain = jnp.where(lane // per_w == w, column, mixer_gain)
     token_w = nn(jnp.concatenate(token_parts, axis=1), window_pick)
-    for k in range(second_fetch, all_fetch):
-        local[k].wait()
-    for copy in ag2_copies:
-        copy.wait_recv()
-    for copy in wo_window:
-        copy.wait_recv()
+    for copy in got_weights:
+        copy.wait()
+    ag2_sent.wait_recv()
+    wo_window.wait_recv()
     everyone = ag2[...].astype(f32).reshape(count * kinds, head).astype(bf16)
     for h in range(heads):
         picked = nn(head_picks[h], everyone).astype(bf16)
@@ -499,12 +502,10 @@
             at = w * out_wide + h * head
             diag[w * per_w : (w + 1) * per_w, at : at + head] = picked
     att[t] = nt(wo_v[...], diag[...]).astype(bf16)
-    copies = to_tp(lambda peer: att.at[t], att, att_s, att_r)
-    pending += copies
-    for copy in copies:
-        copy.wait_recv()
-    for copy in wu_window:
-        copy.wait_recv()
+    att_sent = to_tp(att, att_s, att_r)
+    pending.append(att_sent)
+    att_sent.wait_recv()
+    wu_window.wait_recv()
 
     attended = att[0].astype(f32)
     for k in range(1, n_tp):
@@ -523,22 +524,18 @@
         )
     rs3[...] = product.astype(bf16).reshape(rs3.shape)
     sq_src[...] = jnp.sum(middle * middle, axis=0, keepdims=True)
-    rs3_copies = to_far(lambda i: rs3.at[i], rs3_far, rs3_s, rs3_r, -1)
-    sq_copies = to_far(lambda i: sq_src, sq_far, sq_s, sq_r, -1)
-    pending += rs3_copies + sq_copies
-    mid_copies = []
+    rs3_sent = to_far(lambda i: rs3.at[i], rs3_far, rs3_s, rs3_r, -1)
+    sq_sent = to_far(lambda i: sq_src, sq_far, sq_s, sq_r, -1)
     for w, offset in enumerate(UP_WINDOW):
         placed = nt(middle_b, window_pick[w * all_rows : (w + 1) * all_rows]).astype(bf16)
         mid_src[w] = placed.reshape(n_tp, mine, all_rows)
         if offset:
-            copy = ex.copy(mid_src.at[w, t], mid.at[w], mid_s.at[w], mid_r.at[w], offset)
-            copy.start()
-            mid_copies.append(copy)
+            ex.copy(mid_src.at[w, t], mid.at[w], mid_s, mid_r, offset).start()
         else:
             mid[w] = mid_src[w, t]
-    pending += mid_copies
-    for copy in sq_copies:
-        copy.wait_recv()
+    mid_sent = waiter(mid.at[0 : n_win - 1], mid_s, mid_r)
+    pending.append(mid_sent)
+    sq_sent.wait_recv()
     lane = iota((1, all_rows), 1)
     squares = jnp.zeros((1, all_rows), f32)
     for i in range(count):
@@ -551,54 +548,43 @@
     )
     second = lax.rsqrt(squares / width + epsilon)
     up = jnp.zeros((parts * seq, wide), f32)
-    for copy in reversed(rs3_copies):
-        copy.wait_recv()
+    rs3_sent.wait_recv()
     for i in range(count):
         up += rs3_far[i].astype(f32)
     ag4_src[...] = jnp.square(jnp.maximum(second * up, 0.0)).astype(bf16)
 
-    ag4_copies = to_far(lambda i: ag4_src, ag4, ag4_s, ag4_r, 1)
-    pending += ag4_copies
-    for copy in wdn_window:
-        copy.wait_recv()
-    for copy in mid_copies:
-        copy.wait_recv()
+    ag4_sent = to_far(lambda i: ag4_src, ag4, ag4_s, ag4_r, 1)
+    wdn_window.wait_recv()
+    mid_sent.wait_recv()
     middle = mid[0].astype(f32)
     for w in range(1, n_win):
         middle += mid[w].astype(f32)
-    for copy in ag4_copies:
-        copy.wait_recv()
+    ag4_sent.wait_recv()
     everyone = ag4[...].reshape(count * parts * seq, wide)
     picked = jnp.concatenate(
         [nn(part_picks[j], everyone).astype(bf16) for j in range(parts)], axis=1
     )
     lowered_part = nt(wdn_v[...], picked).astype(bf16)
     fin_src[...] = nn(lowered_part, place_rows).astype(bf16).reshape(fin_src.shape)
-    copies = []
     for w, offset in enumerate(DOWN_WINDOW):
         row = lax.rem(z + offset + n_kv, n_kv)
         for k in range(n_tp):
             if offset == 0 and k == 0:
-                fin[w, t] = fin_src[w, t]
+                fin[w * n_tp + t] = fin_src[w * n_tp + t]
                 continue
             peer = lax.rem(t + k, n_tp)
-            copy = pltpu.make_async_remote_copy(
-                src_ref=fin_src.at[w, peer],
-                dst_ref=fin.at[w, t],
-                send_sem=fin_s.at[w * n_tp + k],
-                recv_sem=fin_r.at[w * n_tp + k],
+            pltpu.make_async_remote_copy(
+                src_ref=fin_src.at[w * n_tp + peer],
+                dst_ref=fin.at[w * n_tp + t],
+                send_sem=fin_s,
+                recv_sem=fin_r,
                 device_id=(g, row, peer),
                 device_id_type=MESH,
-            )
-            copy.start()
-            copies.append(copy)
-    pending += copies
-    for copy in copies:
-        copy.wait_recv()
-    lowered = jnp.zeros((mine, all_rows), f32)
-    for w in range(n_win):
-        for k in range(n_tp):
-            lowered += fin[w, k].astype(f32)
+            ).start()
+    fin_sent = waiter(fin.at[0 : n_win * n_tp - 1], fin_s, fin_r)
+    pending.append(fin_sent)
+    fin_sent.wait_recv()
+    lowered = jnp.sum(fin[...].astype(f32), axis=0)
     out_ref[...] = (middle + lowered).astype(bf16)
     for copy in pending:
         copy.wait_send()
@@ -631,16 +617,13 @@
         wide = w_up.shape[1] // parts
         count = n_kv // 4
         dims = (n_kv, n_tp, seq, heads, block * n_kv)
-        vmem, hbm, smem = (
+        vmem, hbm = (
             pl.BlockSpec(memory_space=pltpu.VMEM),
             pl.BlockSpec(memory_space=pltpu.HBM),
-            pl.BlockSpec(memory_space=pltpu.SMEM),
         )
         dma = pltpu.SemaphoreType.DMA
         blocks = (parts * seq, wide)
         near = (3 * count - 1,)
-        far = (count,)
-        n_local = 3 * heads + 2 + 1 + 3 + 1
         n_win = len(UP_WINDOW)
         scratch = [
             pltpu.VMEM((n_tp + 1, mine, rows), bf16),
@@ -667,31 +650,18 @@
             pltpu.VMEM((count, 1, rows), f32),
             pltpu.VMEM(blocks, bf16),
             pltpu.VMEM((count, *blocks), bf16),
-            pltpu.VMEM((n_win, n_tp, mine, rows), bf16),
-            pltpu.VMEM((n_win, n_tp, mine, rows), bf16),
-            dma((n_local,)),
-            dma((n_tp - 1,)),
-            dma((n_tp - 1,)),
-            dma(near),
-            dma(near),
-            dma(far),
-            dma(far),
-            dma((4 * (n_win - 1),)),
-            dma((4 * (n_win - 1),)),
-            dma(far),
-            dma(far),
-            dma((n_tp - 1,)),
-            dma((n_tp - 1,)),
-            dma(far),
-            dma(far),
-            dma(far),
-            dma(far),
-            dma((n_win,)),
-            dma((n_win,)),
-            dma(far),
-            dma(far),
-            dma((n_win * n_tp,)),
-            dma((n_win * n_tp,)),
+            pltpu.VMEM((n_win * n_tp, mine, rows), bf16),
+            pltpu.VMEM((n_win * n_tp, mine, rows), bf16),
+            pltpu.VMEM(norm_gain.shape, bf16),
+            pltpu.VMEM(mixer_gain.shape, bf16),
+            pltpu.VMEM((1, head), f32),
+            pltpu.VMEM(a_log.shape, f32),
+            pltpu.VMEM(dt_bias.shape, f32),
+            dma((13,)),
+            *[dma] * 6,
+            dma((4,)),
+            dma((4,)),
+            *[dma] * 14,
             pltpu.SemaphoreType.REGULAR,
             pltpu.SemaphoreType.REGULAR,
             pltpu.SemaphoreType.REGULAR,
@@ -702,42 +672,31 @@
                 jax.ShapeDtypeStruct((mine, rows), bf16),
                 jax.ShapeDtypeStruct(state.shape, f32),
             ),
-            in_specs=[
-                vmem,
-                hbm,
-                vmem,
-                hbm,
-                hbm,
-                hbm,
-                hbm,
-                hbm,
-                smem,
-                smem,
-                vmem,
-                hbm,
-                vmem,
-                hbm,
-                hbm,
-            ],
+            in_specs=[hbm] * 15,
             out_specs=(vmem, vmem),
             scratch_shapes=scratch,
             compiler_params=pltpu.CompilerParams(collective_id=0, has_side_effects=True, vmem_limit_bytes=32 * 2**20),
         )(
-            tokens.T,
-            pltpu.with_memory_space_constraint(state, pltpu.HBM),
-            norm_gain,
-            pltpu.with_memory_space_constraint(w_query, pltpu.HBM),
-            pltpu.with_memory_space_constraint(w_key, pltpu.HBM),
-            pltpu.with_memory_space_constraint(w_value, pltpu.HBM),
-            pltpu.with_memory_space_constraint(w_beta.T, pltpu.HBM),
-            pltpu.with_memory_space_constraint(w_decay.T, pltpu.HBM),
-            a_log,
-            dt_bias,
-            head_gain.reshape(1, head),
-            pltpu.with_memory_space_constraint(w_out.T, pltpu.HBM),
-            mixer_gain,
-            pltpu.with_memory_space_constraint(w_up, pltpu.HBM),
-            pltpu.with_memory_space_constraint(w_down.T, pltpu.HBM),
+            *[
+                pltpu.with_memory_space_constraint(x, pltpu.HBM)
+                for x in (
+                    tokens.T,
+                    state,
+                    norm_gain,
+                    w_query,
+                    w_key,
+                    w_value,
+                    w_beta.T,
+                    w_decay.T,
+                    a_log,
+                    dt_bias,
+                    head_gain.reshape(1, head),
+                    w_out.T,
+                    mixer_gain,
+                    w_up,
+                    w_down.T,
+                )
+            ]
         )
         return mixed_t.T, new_state
 

time: 123 us -> 119 us (0.967)
  Pallas kernels: 120 us -> 117 us
    pallas_call x1, Pallas kernels: 120 us -> 117 us  [local(): pl.pallas_call(functools.partial(kernel, dims), out_shape=(jax.ShapeDtype...]
where the time goes in v5:
time: 119 us
  Pallas kernels  117 us (98%)
  local copies, waits for them, and re-layouts  1.37 us (1%)
    pallas_call x1, Pallas kernels, local(): pl.pallas_call(functools.partial(kernel, dims), out_shape=(jax.ShapeDtype...  117 us

profile of v5, /device:TPU:33, one launch (start us, length us, event | category | flops | bytes accessed | tf_op | source)
XLA Modules:
  0.0 118.9 jit_solution(1613268092178407036)
XLA Ops:
  0.6 116.9 %shard_map.158 = (bf16[8,128]{1,0:T(8,128)(2,1)S(1)}, f32[4,2,128,128]{3,2,1,0:T(8,128)S(1)}) custom-call(bf16[8,128]{1,0:T(8,128)(2,1)} %bitcast.12, f32[4,2,128,128]{3,2,1,0:T(8,128)} %state_hbm.1, bf16[64]{0:T(256)(128)(2,1)} %gain_ref.1, bf16[64,256]{1,0:T(8,128)(2,1)} %wq_hbm.1, bf16[64,256]{1,0:T(8,128)(2,1)} %wk_hbm.1, bf16[64,256]{1,0:T(8,128)(2,1)} %wv_hbm.1, ...), custom_call_target="tpu_custom_call" | custom-call | tf_op jit(solution)/shard_map/pallas_call | solution.py:669
  117.6 0.6 copy.19
  118.1 0.8 copy.20

commit v6 on v5

--- a/solution.py
+++ b/solution.py
@@ -167,7 +167,6 @@
     fin_r,
     sem_a,
     sem_b,
-    sem_c,
 ):
     n_kv, n_tp, seq, heads, width = dims
     g, z, t = lax.axis_index("grp"), lax.axis_index("kv"), lax.axis_index("tp")
@@ -185,7 +184,7 @@
     barrier = pltpu.get_barrier_semaphore()
     for k in range(1, n_tp):
         pl.semaphore_signal(barrier, inc=1, device_id=tp_peer(k), device_id_type=MESH)
-    for offset in (1, -1, 2, -2):
+    for offset in (1, -1, 2, -2, 4, -4):
         pl.semaphore_signal(barrier, inc=1, device_id=ex.device(offset), device_id_type=MESH)
 
     def waiter(ref, send, recv):
@@ -259,8 +258,8 @@
     gain = column_of(gain_v[...].astype(f32).reshape(1, block))
     got_tok.wait()
 
-    pl.semaphore_wait(barrier, n_tp - 1 + 4)
-    for offset in (2, -2):
+    pl.semaphore_wait(barrier, n_tp - 1 + 6)
+    for offset in (4, -4):
         pl.semaphore_signal(sem_a, inc=1, device_id=ex.device(offset), device_id_type=MESH)
 
     def to_tp(dst, send, recv):
@@ -297,10 +296,10 @@
     square_t = (at_row == 2 * n_heads).astype(bf16)
     ext_t = jnp.concatenate([wext_t, square_t], axis=1)
 
+    tok_sent.wait_recv()
     pl.semaphore_wait(sem_a, 2)
-    for offset in (4, -4):
+    for offset in (8, -8):
         pl.semaphore_signal(sem_b, inc=1, device_id=ex.device(offset), device_id_type=MESH)
-    tok_sent.wait_recv()
 
     def spread(x_t):
         stacked = jnp.concatenate([x_t] * parts, axis=0)
@@ -326,9 +325,6 @@
             ).start()
     near_sent = waiter(rs1.at[0 : 3 * count - 1], rs1_ns, rs1_nr)
     pending.append(near_sent)
-    pl.semaphore_wait(sem_b, 2)
-    for offset in (8, -8):
-        pl.semaphore_signal(sem_c, inc=1, device_id=ex.device(offset), device_id_type=MESH)
     near_sent.wait_recv()
     for i in range(count):
         total = rs1[2 * count + i].astype(f32)
@@ -336,7 +332,7 @@
             k = group * count + i if group < 2 else 2 * count + i
             total += rs1_near[k].astype(f32)
         rs1_far_src[i] = total.astype(bf16)
-    pl.semaphore_wait(sem_c, 2)
+    pl.semaphore_wait(sem_b, 2)
 
     def to_far(src_of, dst, send, recv, sign):
         for i in ex.farthest_first:
@@ -664,7 +660,6 @@
             *[dma] * 14,
             pltpu.SemaphoreType.REGULAR,
             pltpu.SemaphoreType.REGULAR,
-            pltpu.SemaphoreType.REGULAR,
         ]
         mixed_t, new_state = pl.pallas_call(
             functools.partial(kernel, dims),

time: 119 us -> 118 us (level)
    pallas_call x1, Pallas kernels: 117 us -> 116 us  [local(): pl.pallas_call(functools.partial(kernel, dims), out_shape=(jax.ShapeDtype...]
where the time goes in v6:
time: 118 us
  Pallas kernels  116 us (98%)
  local copies, waits for them, and re-layouts  1.37 us (1%)
    pallas_call x1, Pallas kernels, local(): pl.pallas_call(functools.partial(kernel, dims), out_shape=(jax.ShapeDtype...  116 us

profile of v6, /device:TPU:33, one launch (start us, length us, event | category | flops | bytes accessed | tf_op | source)
XLA Modules:
  0.0 117.7 jit_solution(11086378197677175912)
XLA Ops:
  0.6 115.6 %shard_map.158 = (bf16[8,128]{1,0:T(8,128)(2,1)S(1)}, f32[4,2,128,128]{3,2,1,0:T(8,128)S(1)}) custom-call(bf16[8,128]{1,0:T(8,128)(2,1)} %bitcast.12, f32[4,2,128,128]{3,2,1,0:T(8,128)} %state_hbm.1, bf16[64]{0:T(256)(128)(2,1)} %gain_ref.1, bf16[64,256]{1,0:T(8,128)(2,1)} %wq_hbm.1, bf16[64,256]{1,0:T(8,128)(2,1)} %wk_hbm.1, bf16[64,256]{1,0:T(8,128)(2,1)} %wv_hbm.1, ...), custom_call_target="tpu_custom_call" | custom-call | tf_op jit(solution)/shard_map/pallas_call | solution.py:664
  116.3 0.6 copy.19
  116.9 0.8 copy.20

commit v7 on v6

--- a/solution.py
+++ b/solution.py
@@ -263,7 +263,7 @@
         pl.semaphore_signal(sem_a, inc=1, device_id=ex.device(offset), device_id_type=MESH)
 
     def to_tp(dst, send, recv):
-        for k in range(1, n_tp):
+        for k in sorted(range(1, n_tp), key=lambda k: -min(k, n_tp - k)):
             peer = lax.rem(t + k, n_tp)
             pltpu.make_async_remote_copy(
                 src_ref=dst.at[t],
@@ -317,31 +317,50 @@
     product = jnp.concatenate([product[:, :head], product[:, head:] + extra], axis=1)
     rs1[...] = product.astype(bf16).reshape(rs1.shape)
 
-    for i in ex.farthest_first:
-        for group, step in ex.near(i):
-            k = group * count + i if group < 2 else 2 * count + i
-            ex.copy(
-                rs1.at[group * count + i], rs1_near.at[k], rs1_ns, rs1_nr, -step
-            ).start()
-    near_sent = waiter(rs1.at[0 : 3 * count - 1], rs1_ns, rs1_nr)
-    pending.append(near_sent)
-    near_sent.wait_recv()
-    for i in range(count):
-        total = rs1[2 * count + i].astype(f32)
-        for group, step in ex.near(i):
-            k = group * count + i if group < 2 else 2 * count + i
-            total += rs1_near[k].astype(f32)
-        rs1_far_src[i] = total.astype(bf16)
-    pl.semaphore_wait(sem_b, 2)
-
-    def to_far(src_of, dst, send, recv, sign):
-        for i in ex.farthest_first:
+    def to_far(chosen, src_of, dst, send, recv, sign):
+        for i in chosen:
             ex.copy(src_of(i), dst.at[i], send, recv, sign * ex.reach[i]).start()
+
+    def far_waiter(dst, send, recv):
         sent = waiter(dst, send, recv)
         pending.append(sent)
         return sent
 
-    far_sent = to_far(lambda i: rs1_far_src.at[i], rs1_far, rs1_fs, rs1_fr, -1)
+    distant, close = ex.farthest_first[:count // 2], ex.farthest_first[count // 2 :]
+
+    near_sent = []
+    for part, chosen in enumerate((distant, close)):
+        started = 0
+        for i in chosen:
+            for group, step in ex.near(i):
+                k = group * count + i if group < 2 else 2 * count + i
+                ex.copy(
+                    rs1.at[group * count + i],
+                    rs1_near.at[k],
+                    rs1_ns.at[part],
+                    rs1_nr.at[part],
+                    -step,
+                ).start()
+                started += 1
+        near_sent.append(waiter(rs1.at[0:started], rs1_ns.at[part], rs1_nr.at[part]))
+    pending += near_sent
+
+    def near_sums(chosen):
+        for i in chosen:
+            total = rs1[2 * count + i].astype(f32)
+            for group, step in ex.near(i):
+                k = group * count + i if group < 2 else 2 * count + i
+                total += rs1_near[k].astype(f32)
+            rs1_far_src[i] = total.astype(bf16)
+
+    near_sent[0].wait_recv()
+    near_sums(distant)
+    pl.semaphore_wait(sem_b, 2)
+    to_far(distant, lambda i: rs1_far_src.at[i], rs1_far, rs1_fs, rs1_fr, -1)
+    near_sent[1].wait_recv()
+    near_sums(close)
+    to_far(close, lambda i: rs1_far_src.at[i], rs1_far, rs1_fs, rs1_fr, -1)
+    far_sent = far_waiter(rs1_far, rs1_fs, rs1_fr)
 
     def to_window(src, dst_of, whole, k, offsets):
         for w, offset in enumerate(offsets):
@@ -415,7 +434,14 @@
     )
 
     ag2_src[...] = normed.astype(bf16)
-    ag2_sent = to_far(lambda i: ag2_src, ag2, ag2_s, ag2_r, 1)
+    to_far(distant, lambda i: ag2_src, ag2, ag2_s, ag2_r, 1)
+    for k in range(rows):
+        matrix = state_v[k % seq, k // seq]
+        state_out[k % seq, k // seq] = (
+            decay[k : k + 1] * matrix + key_t[:, k : k + 1] * fresh[k : k + 1]
+        )
+    to_far(close, lambda i: ag2_src, ag2, ag2_s, ag2_r, 1)
+    ag2_sent = far_waiter(ag2, ag2_s, ag2_r)
     wu_window = to_window(
         wu_hbm,
         lambda w: wu_v.at[w * block : (w + 1) * block],
@@ -430,11 +456,6 @@
         3,
         DOWN_WINDOW,
     )
-    for k in range(rows):
-        matrix = state_v[k % seq, k // seq]
-        state_out[k % seq, k // seq] = (
-            decay[k : k + 1] * matrix + key_t[:, k : k + 1] * fresh[k : k + 1]
-        )
 
     def iota(shape, dim):
         return lax.broadcasted_iota(jnp.int32, shape, dim)
@@ -508,6 +529,9 @@
         attended += att[k].astype(f32)
     middle_b = (token_w + attended).astype(bf16)
     middle = middle_b.astype(f32)
+    sq_src[...] = jnp.sum(middle * middle, axis=0, keepdims=True)
+    to_far(ex.farthest_first, lambda i: sq_src, sq_far, sq_s, sq_r, -1)
+    sq_sent = far_waiter(sq_far, sq_s, sq_r)
     scaled = jnp.concatenate([middle * mixer_gain] * n_win, axis=0)
     shape = scaled.shape
     scaled = jnp.where(iota(shape, 1) // per_w == iota(shape, 0) // block, scaled, 0.0)
@@ -519,16 +543,17 @@
             jnp.where(part == j, left, 0.0).astype(bf16), wu_v[:, j * wide : (j + 1) * wide]
         )
     rs3[...] = product.astype(bf16).reshape(rs3.shape)
-    sq_src[...] = jnp.sum(middle * middle, axis=0, keepdims=True)
-    rs3_sent = to_far(lambda i: rs3.at[i], rs3_far, rs3_s, rs3_r, -1)
-    sq_sent = to_far(lambda i: sq_src, sq_far, sq_s, sq_r, -1)
+    to_far(distant, lambda i: rs3.at[i], rs3_far, rs3_s, rs3_r, -1)
     for w, offset in enumerate(UP_WINDOW):
         placed = nt(middle_b, window_pick[w * all_rows : (w + 1) * all_rows]).astype(bf16)
         mid_src[w] = placed.reshape(n_tp, mine, all_rows)
+        if not offset:
+            mid[w] = mid_src[w, t]
+    to_far(close, lambda i: rs3.at[i], rs3_far, rs3_s, rs3_r, -1)
+    rs3_sent = far_waiter(rs3_far, rs3_s, rs3_r)
+    for w, offset in enumerate(UP_WINDOW):
         if offset:
             ex.copy(mid_src.at[w, t], mid.at[w], mid_s, mid_r, offset).start()
-        else:
-            mid[w] = mid_src[w, t]
     mid_sent = waiter(mid.at[0 : n_win - 1], mid_s, mid_r)
     pending.append(mid_sent)
     sq_sent.wait_recv()
@@ -549,12 +574,14 @@
         up += rs3_far[i].astype(f32)
     ag4_src[...] = jnp.square(jnp.maximum(second * up, 0.0)).astype(bf16)
 
-    ag4_sent = to_far(lambda i: ag4_src, ag4, ag4_s, ag4_r, 1)
+    to_far(distant, lambda i: ag4_src, ag4, ag4_s, ag4_r, 1)
     wdn_window.wait_recv()
     mid_sent.wait_recv()
     middle = mid[0].astype(f32)
     for w in range(1, n_win):
         middle += mid[w].astype(f32)
+    to_far(close, lambda i: ag4_src, ag4, ag4_s, ag4_r, 1)
+    ag4_sent = far_waiter(ag4, ag4_s, ag4_r)
     ag4_sent.wait_recv()
     everyone = ag4[...].reshape(count * parts * seq, wide)
     picked = jnp.concatenate(
@@ -562,9 +589,9 @@
     )
     lowered_part = nt(wdn_v[...], picked).astype(bf16)
     fin_src[...] = nn(lowered_part, place_rows).astype(bf16).reshape(fin_src.shape)
-    for w, offset in enumerate(DOWN_WINDOW):
+    for w, offset in sorted(enumerate(DOWN_WINDOW), key=lambda pair: -abs(pair[1])):
         row = lax.rem(z + offset + n_kv, n_kv)
-        for k in range(n_tp):
+        for k in sorted(range(n_tp), key=lambda k: -min(k, n_tp - k)):
             if offset == 0 and k == 0:
                 fin[w * n_tp + t] = fin_src[w * n_tp + t]
                 continue
@@ -654,7 +681,12 @@
             pltpu.VMEM(a_log.shape, f32),
             pltpu.VMEM(dt_bias.shape, f32),
             dma((13,)),
-            *[dma] * 6,
+            dma,
+            dma,
+            dma((2,)),
+            dma((2,)),
+            dma,
+            dma,
             dma((4,)),
             dma((4,)),
             *[dma] * 14,

time: 118 us -> 117 us (level)
  Pallas kernels: 116 us -> 114 us
    pallas_call x1, Pallas kernels: 116 us -> 114 us  [local(): pl.pallas_call(functools.partial(kernel, dims), out_shape=(jax.ShapeDtype...]
where the time goes in v7:
time: 117 us; the launch traced here: 116 us
  Pallas kernels  114 us (97%)
  local copies, waits for them, and re-layouts  1.37 us (1%)
    pallas_call x1, Pallas kernels, local(): pl.pallas_call(functools.partial(kernel, dims), out_shape=(jax.ShapeDtype...  114 us

profile of v7, /device:TPU:33, one launch (start us, length us, event | category | flops | bytes accessed | tf_op | source)
XLA Modules:
  0.0 116.4 jit_solution(493619028099238947)
XLA Ops:
  0.6 114.3 %shard_map.158 = (bf16[8,128]{1,0:T(8,128)(2,1)S(1)}, f32[4,2,128,128]{3,2,1,0:T(8,128)S(1)}) custom-call(bf16[8,128]{1,0:T(8,128)(2,1)} %bitcast.12, f32[4,2,128,128]{3,2,1,0:T(8,128)} %state_hbm.1, bf16[64]{0:T(256)(128)(2,1)} %gain_ref.1, bf16[64,256]{1,0:T(8,128)(2,1)} %wq_hbm.1, bf16[64,256]{1,0:T(8,128)(2,1)} %wk_hbm.1, bf16[64,256]{1,0:T(8,128)(2,1)} %wv_hbm.1, ...), custom_call_target="tpu_custom_call" | custom-call | tf_op jit(solution)/shard_map/pallas_call | solution.py:696
  115.0 0.6 copy.19
  115.6 0.8 copy.20

commit v8 on v7

--- a/solution.py
+++ b/solution.py
@@ -44,25 +44,34 @@
 DOWN_WINDOW = (-2, -1, 0, 1)
 
 
+def reach_of(i, n_kv, where=jnp.where):
+    q, top = n_kv // 16, n_kv // 2 - 2
+    return where(i < q, top - 4 * i, where(i < 2 * q, -2 - 4 * i, top + 4 * q - 4 * i))
+
+
 class Exchange:
     def __init__(self, n_kv, g, z, t):
         self.n_kv, self.g, self.z, self.t = n_kv, g, z, t
-        self.half = n_kv // 8
-        up = [2 + 4 * i for i in range(self.half)]
-        self.reach = up + [-u for u in up]
-        self.count = 2 * self.half
-        self.steps = [(0, 1), (1, -1)]
-        self.farthest_first = [
-            k * self.half + i for i in reversed(range(self.half)) for k in (0, 1)
+        self.count = n_kv // 4
+        self.reach = [
+            reach_of(i, n_kv, lambda c, x, y: x if c else y) for i in range(self.count)
         ]
-        self.nearest_first = list(reversed(self.farthest_first))
+        self.farthest_first = sorted(range(self.count), key=lambda i: -abs(self.reach[i]))
+        self.own = 3 * self.count + n_kv // 8 - 1
 
     def device(self, offset):
         return (self.g, lax.rem(self.z + offset + self.n_kv, self.n_kv), self.t)
 
-    def near(self, i):
-        last = () if i == self.count - 1 else ((3, 2 if i < self.half else -2),)
-        return self.steps + list(last)
+    def near_runs(self):
+        q = self.n_kv // 16
+        farther = [(3, 0, q, 2), (3, q, q - 1, -2), (0, 0, 2 * q, 1), (1, 0, 2 * q, -1)]
+        closer = [
+            (3, 2 * q, q, 2),
+            (3, 3 * q, q, -2),
+            (0, 2 * q, 2 * q, 1),
+            (1, 2 * q, 2 * q, -1),
+        ]
+        return farther, closer
 
     def copy(self, src, dst, send, recv, offset):
         return pltpu.make_async_remote_copy(
@@ -77,16 +86,15 @@
 
 def placing(per_slot, n_kv, seq, z):
     count = n_kv // 4
-    half = count // 2
     shape = (n_kv * per_slot, n_kv * seq)
     m = lax.broadcasted_iota(jnp.int32, shape, 0)
     slot = m // per_slot
     i = slot % count
     group = slot // count
-    reach = jnp.where(i < half, 2 + 4 * i, 4 * half - 2 - 4 * i)
-    side = jnp.where(i < half, 2, -2)
+    reach = reach_of(i, n_kv)
+    side = jnp.where(reach > 0, 2, -2)
     step = jnp.where(group == 0, 1, jnp.where(group == 1, -1, jnp.where(group == 2, 0, side)))
-    offset = jnp.where(slot == n_kv - 1, 0, reach + step)
+    offset = jnp.where(slot == 3 * count + n_kv // 8 - 1, 0, reach + step)
     owner = (z - offset + n_kv) % n_kv
     row = owner * seq + m % seq
     return (row == lax.broadcasted_iota(jnp.int32, shape, 1)).astype(bf16)
@@ -171,12 +179,12 @@
     n_kv, n_tp, seq, heads, width = dims
     g, z, t = lax.axis_index("grp"), lax.axis_index("kv"), lax.axis_index("tp")
     ex = Exchange(n_kv, g, z, t)
-    count, half = ex.count, ex.half
+    count = ex.count
     mine = tok_ref.shape[0]
     block = n_tp * mine
     all_rows = tok_ref.shape[1]
     head = hgain_v.shape[1]
-    own = n_kv - 1
+    own = ex.own
 
     def tp_peer(k):
         return (g, z, lax.rem(t + k, n_tp))
@@ -329,28 +337,26 @@
     distant, close = ex.farthest_first[:count // 2], ex.farthest_first[count // 2 :]
 
     near_sent = []
-    for part, chosen in enumerate((distant, close)):
-        started = 0
-        for i in chosen:
-            for group, step in ex.near(i):
-                k = group * count + i if group < 2 else 2 * count + i
-                ex.copy(
-                    rs1.at[group * count + i],
-                    rs1_near.at[k],
-                    rs1_ns.at[part],
-                    rs1_nr.at[part],
-                    -step,
-                ).start()
-                started += 1
-        near_sent.append(waiter(rs1.at[0:started], rs1_ns.at[part], rs1_nr.at[part]))
+    for part, runs in enumerate(ex.near_runs()):
+        for group, first, blocks, step in runs:
+            at, to = group * count + first, min(group, 2) * count + first
+            ex.copy(
+                rs1.at[at : at + blocks],
+                rs1_near.at[to : to + blocks],
+                rs1_ns.at[part],
+                rs1_nr.at[part],
+                -step,
+            ).start()
+        blocks = sum(run[2] for run in runs)
+        near_sent.append(waiter(rs1.at[0:blocks], rs1_ns.at[part], rs1_nr.at[part]))
     pending += near_sent
 
     def near_sums(chosen):
         for i in chosen:
             total = rs1[2 * count + i].astype(f32)
-            for group, step in ex.near(i):
-                k = group * count + i if group < 2 else 2 * count + i
-                total += rs1_near[k].astype(f32)
+            for k in range(3):
+                if k < 2 or 3 * count + i != own:
+                    total += rs1_near[k * count + i].astype(f32)
             rs1_far_src[i] = total.astype(bf16)
 
     near_sent[0].wait_recv()
@@ -461,9 +467,7 @@
         return lax.broadcasted_iota(jnp.int32, shape, dim)
 
     def owner_row(slot, r):
-        half = ex.half
-        reach = jnp.where(slot < half, 2 + 4 * slot, 4 * half - 2 - 4 * slot)
-        return (z - reach + n_kv) % n_kv * seq + r
+        return (z - reach_of(slot, n_kv) + n_kv) % n_kv * seq + r
 
     per_w = count * seq
     shape = (n_win * all_rows, all_rows)
@@ -646,7 +650,6 @@
         )
         dma = pltpu.SemaphoreType.DMA
         blocks = (parts * seq, wide)
-        near = (3 * count - 1,)
         n_win = len(UP_WINDOW)
         scratch = [
             pltpu.VMEM((n_tp + 1, mine, rows), bf16),
@@ -658,7 +661,7 @@
             pltpu.VMEM((n_win * block, w_up.shape[1]), bf16),
             pltpu.VMEM((n_win * block, w_down.shape[0]), bf16),
             pltpu.VMEM((n_kv, *blocks), bf16),
-            pltpu.VMEM((*near, *blocks), bf16),
+            pltpu.VMEM((3 * count, *blocks), bf16),
             pltpu.VMEM((count, *blocks), bf16),
             pltpu.VMEM((count, *blocks), bf16),
             pltpu.VMEM((heads * seq, head), bf16),

time: 117 us -> 117 us (level)
  no operation moved by 1% of the time
where the time goes in v8:
time: 117 us
  Pallas kernels  115 us (98%)
  local copies, waits for them, and re-layouts  1.37 us (1%)
    pallas_call x1, Pallas kernels, local(): pl.pallas_call(functools.partial(kernel, dims), out_shape=(jax.ShapeDtype...  115 us

profile of v8, /device:TPU:33, one launch (start us, length us, event | category | flops | bytes accessed | tf_op | source)
XLA Modules:
  0.0 116.6 jit_solution(14514632097484984404)
XLA Ops:
  0.6 114.6 %shard_map.158 = (bf16[8,128]{1,0:T(8,128)(2,1)S(1)}, f32[4,2,128,128]{3,2,1,0:T(8,128)S(1)}) custom-call(bf16[8,128]{1,0:T(8,128)(2,1)} %bitcast.12, f32[4,2,128,128]{3,2,1,0:T(8,128)} %state_hbm.1, bf16[64]{0:T(256)(128)(2,1)} %gain_ref.1, bf16[64,256]{1,0:T(8,128)(2,1)} %wq_hbm.1, bf16[64,256]{1,0:T(8,128)(2,1)} %wk_hbm.1, bf16[64,256]{1,0:T(8,128)(2,1)} %wv_hbm.1, ...), custom_call_target="tpu_custom_call" | custom-call | tf_op jit(solution)/shard_map/pallas_call | solution.py:699
  115.2 0.6 copy.19
  115.8 0.8 copy.20

commit v9 on v8

--- a/solution.py
+++ b/solution.py
@@ -615,6 +615,17 @@
     out_ref[...] = (middle + lowered).astype(bf16)
     for copy in pending:
         copy.wait_send()
+
+
+def write_out(mixed_ref, state_ref, mixed_out, state_out, sems):
+    copies = [
+        pltpu.make_async_copy(state_ref, state_out, sems.at[0]),
+        pltpu.make_async_copy(mixed_ref, mixed_out, sems.at[1]),
+    ]
+    for copy in copies:
+        copy.start()
+    for copy in copies:
+        copy.wait()
 
 
 def solution(mesh):
@@ -728,6 +739,17 @@
                 )
             ]
         )
+        mixed_t, new_state = pl.pallas_call(
+            write_out,
+            out_shape=(
+                jax.ShapeDtypeStruct((mine, rows), bf16),
+                jax.ShapeDtypeStruct(state.shape, f32),
+            ),
+            in_specs=[vmem, vmem],
+            out_specs=(hbm, hbm),
+            scratch_shapes=[dma((2,))],
+            compiler_params=pltpu.CompilerParams(vmem_limit_bytes=2**20),
+        )(mixed_t, new_state)
         return mixed_t.T, new_state
 
     return jax.shard_map(

time: 117 us -> 116 us (level)
  local copies, waits for them, and re-layouts: 1.37 us -> 0 us
    unnamed x2 -> x0, local copies, waits for them, and re-layouts: 1.37 us -> none
where the time goes in v9:
time: 116 us
  Pallas kernels  115 us (99%)
    pallas_call x1, Pallas kernels, local(): pl.pallas_call(functools.partial(kernel, dims), out_shape=(jax.ShapeDtype...  115 us

profile of v9, /device:TPU:33, one launch (start us, length us, event | category | flops | bytes accessed | tf_op | source)
XLA Modules:
  0.0 116.0 jit_solution(10463323720677752275)
XLA Ops:
  0.6 114.6 %shard_map.158 = (bf16[8,128]{1,0:T(8,128)(2,1)S(1)}, f32[4,2,128,128]{3,2,1,0:T(8,128)S(1)}) custom-call(bf16[8,128]{1,0:T(8,128)(2,1)} %bitcast.11, f32[4,2,128,128]{3,2,1,0:T(8,128)} %state_hbm.1, bf16[64]{0:T(256)(128)(2,1)} %gain_ref.1, bf16[64,256]{1,0:T(8,128)(2,1)} %wq_hbm.1, bf16[64,256]{1,0:T(8,128)(2,1)} %wk_hbm.1, bf16[64,256]{1,0:T(8,128)(2,1)} %wv_hbm.1, ...), custom_call_target="tpu_custom_call" | custom-call | tf_op jit(solution)/shard_map/pallas_call | solution.py:710
  115.2 0.8 shard_map.159
